TPU v7x, 768 devices: a whole 4x8x12 slice. The times are simulated.
768 devices in a mesh: sp: 192 (over z, y, core), tp: 4 (over x).
Axes of the slice: x: 4, y: 8, z: 12, core: 2. Of those that a mesh axis runs over, the one named last changes fastest.
Arguments:
- query_latent: bfloat16 [49152, 1024], P('sp'), may hold values from -6 to 6
- shared_latent: bfloat16 [49152, 512], P('sp'), may hold values from -25 to 25
- rotary_key: bfloat16 [49152, 64], P('sp'), may hold values from -300 to 300
- document_start: int32 [49152], P('sp'), may hold values from 0 to 49151, as said below
- query_gain: float32 [1024], replicated, may hold values from 0.1 to 1.9
- shared_gain: float32 [512], replicated, may hold values from 0.1 to 1.9
- content_weight: bfloat16 [1024, 2048], P(None, 'tp'), may hold values from -0.1875 to 0.1875
- rotary_weight: bfloat16 [1024, 1024], P(None, 'tp'), may hold values from -0.1875 to 0.1875
- key_weight: bfloat16 [512, 2048], P(None, 'tp'), may hold values from -0.25 to 0.25
- value_weight: bfloat16 [512, 2048], P(None, 'tp'), may hold values from -0.25 to 0.25
- output_weight: bfloat16 [2048, 4096], P('tp'), may hold values from -0.125 to 0.125
Outputs:
- mixed: bfloat16 [49152, 4096], P('sp')
Inputs may be any that keep to these rules, and one draw needn't show every extreme that they name: `document_start`: each position holds the first position of its document; documents are runs of 1 to 1792 consecutive positions and one of them has exactly 1792; the values never fall.
All inputs are finite; a program needn't handle non-finite values.
Results may differ from a plain program's by a relative error of at most 0.038.
The roundings to bfloat16 on the way count: a program that leaves them out, or rounds other values in their place, can miss the bound.
Values may be sent and summed in bfloat16 or wider, within the bound.
A program may use at most 64 MiB of HBM per device.

v0:
```python
import jax
import jax.numpy as jnp
from jax import lax
from jax.sharding import PartitionSpec as P

MODEL = 4096
CONTENT = 128
ROTARY = 64
VALUE_DIM = 128
SPAN = 8


norm_eps = 1e-06
rope_theta = 10000.0
masked_score = -1e30


def from_behind(value, axis, steps):
    count = lax.axis_size(axis)
    initial, last = (max(0, -steps), min(count, count - steps))
    return lax.ppermute(value, axis, [(source, source + steps) for source in range(initial, last)])


def rms_scale(latent, scaling):
    entries = latent.astype(jnp.float32)
    scaled = entries * lax.rsqrt(jnp.mean(entries * entries, axis=-1, keepdims=True) + norm_eps)
    return (scaled * scaling).astype(jnp.bfloat16)


def rotate(entries, places):
    width = entries.shape[-1]
    halfway = width // 2
    frequency = 1.0 / rope_theta ** (jnp.arange(0, width, 2, dtype=jnp.float32) / width)
    angles = places.astype(jnp.float32)[:, None] * frequency[None, :]
    target = (angles.shape[0],) + (1,) * (entries.ndim - 2) + (halfway,)
    cosine_table = jnp.cos(angles).reshape(target)
    sine_table = jnp.sin(angles).reshape(target)
    leading = entries[..., :halfway]
    trailing = entries[..., halfway:]
    return jnp.concatenate(
        [
            leading * cosine_table - trailing * sine_table,
            leading * sine_table + trailing * cosine_table,
        ],
        axis=-1,
    )


def expand(shared_block, key_weight, value_weight):
    expanded_keys = jnp.dot(shared_block, key_weight, preferred_element_type=jnp.float32).astype(
        jnp.bfloat16
    )
    expanded_values = jnp.dot(
        shared_block, value_weight, preferred_element_type=jnp.float32
    ).astype(jnp.bfloat16)
    return (expanded_keys, expanded_values)


def on_device(
    query_latent,
    shared_latent,
    rotary_key,
    document_start,
    query_gain,
    shared_gain,
    content_weight,
    rotary_weight,
    key_weight,
    value_weight,
    output_weight,
):
    length = query_latent.shape[0]
    anchor = lax.axis_index("sp") * length
    head_count = key_weight.shape[1] // CONTENT
    places = anchor + jnp.arange(length, dtype=jnp.int32)
    query_rows = rms_scale(query_latent, query_gain)
    shared_rows = rms_scale(shared_latent, shared_gain)
    turn_rows = rotate(rotary_key.astype(jnp.float32), places).astype(jnp.bfloat16)
    query_content = (
        jnp.dot(query_rows, content_weight, preferred_element_type=jnp.float32)
        .astype(jnp.bfloat16)
        .reshape(length, head_count, CONTENT)
    )
    query_raw = jnp.dot(query_rows, rotary_weight, preferred_element_type=jnp.float32).reshape(
        length, head_count, ROTARY
    )
    query_turn = rotate(query_raw, places).astype(jnp.bfloat16)
    first_start = document_start[0]
    score_scale = (CONTENT + ROTARY) ** (-0.5)
    payload = (shared_rows, turn_rows)

    def absorb(softmax_state, arrived, distance):
        block_anchor = anchor - distance * length

        def update(current):
            block_shared, block_turn = arrived
            block_keys, block_values = expand(block_shared, key_weight, value_weight)
            block_keys = block_keys.reshape(length, head_count, CONTENT)
            block_values = block_values.reshape(length, head_count, VALUE_DIM)
            scores = jnp.einsum(
                "qhd,khd->hqk", query_content, block_keys, preferred_element_type=jnp.float32
            )
            scores = scores + jnp.einsum(
                "qhr,kr->hqk", query_turn, block_turn, preferred_element_type=jnp.float32
            )
            key_places = block_anchor + jnp.arange(length, dtype=jnp.int32)
            visible = (key_places[None, :] >= document_start[:, None]) & (
                key_places[None, :] <= places[:, None]
            )
            scores = jnp.where(visible[None], scores * score_scale, masked_score)
            running, denominator, summed = current
            highest = jnp.maximum(running, jnp.max(scores, axis=-1))
            factor = jnp.exp(running - highest)
            weights = jnp.exp(scores - highest[:, :, None])
            denominator = denominator * factor + jnp.sum(weights, axis=-1)
            summed = summed * factor[:, :, None] + jnp.einsum(
                "hqk,khd->hqd",
                weights.astype(jnp.bfloat16),
                block_values,
                preferred_element_type=jnp.float32,
            )
            return (highest, denominator, summed)

        def unchanged(current):
            return current

        needed = (block_anchor >= 0) & (block_anchor + length - 1 >= first_start)
        return lax.cond(needed, update, unchanged, softmax_state)

    initial = (
        jnp.full((head_count, length), masked_score, jnp.float32),
        jnp.zeros((head_count, length), jnp.float32),
        jnp.zeros((head_count, length, VALUE_DIM), jnp.float32),
    )
    softmax_state = absorb(initial, payload, 0)

    def advance(counter, carried):
        moving, current = carried
        moving = from_behind((moving[0], moving[1]), "sp", 1)
        return (moving, absorb(current, moving, counter + 1))

    moving, softmax_state = lax.fori_loop(0, SPAN - 1, advance, (payload, softmax_state))
    highest, denominator, summed = softmax_state
    attended = (summed / denominator[:, :, None]).astype(jnp.bfloat16)
    weight_heads = output_weight.reshape(head_count, VALUE_DIM, MODEL)
    group_term = jnp.einsum(
        "hqd,hdm->qm", attended, weight_heads, preferred_element_type=jnp.float32
    ).astype(jnp.bfloat16)
    group_term = lax.optimization_barrier(group_term).astype(jnp.float32)
    mixed = lax.psum(group_term.astype(jnp.bfloat16), "tp")
    return mixed


def solution(mesh):
    return jax.shard_map(
        on_device,
        mesh=mesh,
        in_specs=(
            P("sp", None),
            P("sp", None),
            P("sp", None),
            P("sp"),
            P(),
            P(),
            P(None, "tp"),
            P(None, "tp"),
            P(None, "tp"),
            P(None, "tp"),
            P("tp", None),
        ),
        out_specs=P("sp", None),
        check_vma=False,
    )
```

profile of v0, /device:TPU:1, one launch (start us, length us, event | category | flops | bytes accessed | tf_op | source)
XLA Modules:
  0.0 215.6 jit_solution(12606637039265560594)
XLA Ops:
  6.7 1.4 fusion.33
  8.1 1.5 convolution_convert_fusion.4
  9.7 1.3 slice.17
  11.7 1.1 fusion.36
  12.8 1.6 fusion.40
  15.6 6.6 %conditional.2 = (f32[4,256]{1,0:T(4,128)}, f32[4,256]{1,0:T(4,128)S(1)}, f32[4,256,128]{2,1,0:T(8,128)S(1)}) conditional(s32[]{:T(128)} %convert_element_type.74, () %tuple.50, (s32[]{:T(128)}, s32[256]{0:T(256)S(1)}, s32[256]{0:T(256)S(1)}, bf16[256,512]{1,0:T(8,128)(2,1)}, bf16[512,512]{1,0:T(8,128)(2,1)S(1)}, ...), branch_computations={%region_2.0_spmd, %region_3.6_spmd} | conditional | flops 438898944 | bytes 8994844 | solution.py:128
  15.8 1.3 fusion.6
  17.0 1.2 fusion.5
  20.4 1.1 convolution_add_fusion
  22.2 80.4 %while.27 = (s32[]{:T(128)}, bf16[256,512]{1,0:T(8,128)(2,1)}, bf16[256,64]{0,1:T(8,128)(2,1)S(1)}, f32[4,256]{1,0:T(4,128)}, f32[4,256]{1,0:T(4,128)S(1)}, /*in...) while((s32[]{:T(128)}, bf16[256,512]{1,0:T(8,128)(2,1)}, ...), condition=%wide.region_11.12_spmd.clone.clone, body=%wide.region_6.11_spmd.clone.clone.sunk | while | flops 439028224 | bytes 11312595 | solution.py:142
  22.2 4.6 %collective-permute-start = (bf16[256,512]{1,0:T(8,128)(2,1)}, bf16[256,512]{1,0:T(8,128)(2,1)S(1)}, u32[]{:S(2)}, u32[]{:S(2)}) collective-permute-start(bf16[256,512]{1,0:T(8,128)(2,1)} %get-tuple-element.794), channel_id=1, source_target_pairs={{0,4},{4,8},{8,12},{12,16},{16,20},{20,24},{24,28},{28,32},{32,36}... | collective-permute-start | bytes 786440 | tf_op jit(solution)/shard_map/while/body/eval_jaxpr/ppermute | solution.py:21
  26.8 1.9 collective-permute-start.1
  29.4 6.5 %collective-permute-done.1 = bf16[256,64]{0,1:T(8,128)(2,1)S(1)} collective-permute-done((bf16[256,64]{0,1:T(8,128)(2,1)S(1)}, bf16[256,64]{0,1:T(8,128)(2,1)S(1)}, u32[]{:S(2)}, u32[]{:S(2)}) %collective-permute-start.1) | collective-permute-done | bytes 32800 | tf_op jit(solution)/shard_map/while/body/eval_jaxpr/ppermute | solution.py:21
  35.9 4.1 %conditional.6 = ((f32[4,256]{1,0:T(4,128)}, f32[4,256]{1,0:T(4,128)S(1)}, f32[4,256,128]{2,1,0:T(8,128)S(1)})) conditional(s32[]{:T(128)} %convert_element_type.126, (f32[4,256]{1,0:T(4,128)}, f32[4,256]{1,0:T(4,128)S(1)}, f32[4,256,128]{2,1,0:T(8,128)S(1)}) %tuple.86, (s32[]{:T(128)}, s32[256]{0:T(256)S(1)}, s32[]{:T(128)}, ...), branch_computations={%region_7.7_spmd, %region_8.10_spmd} | conditional | flops 439028224 | bytes 9541672 | solution.py:128
  40.7 1.9 collective-permute-start
  42.6 1.9 collective-permute-start.1
  45.3 1.2 collective-permute-done.1
  47.2 8.4 %collective-permute-start = (bf16[256,512]{1,0:T(8,128)(2,1)}, bf16[256,512]{1,0:T(8,128)(2,1)S(1)}, u32[]{:S(2)}, u32[]{:S(2)}) collective-permute-start(bf16[256,512]{1,0:T(8,128)(2,1)} %get-tuple-element.794), channel_id=1, source_target_pairs={{0,4},{4,8},{8,12},{12,16},{16,20},{20,24},{24,28},{28,32},{32,36}... | collective-permute-start | bytes 786440 | tf_op jit(solution)/shard_map/while/body/eval_jaxpr/ppermute | solution.py:21
  55.7 1.9 collective-permute-start.1
  58.3 1.2 collective-permute-done.1
  60.3 4.4 %collective-permute-start = (bf16[256,512]{1,0:T(8,128)(2,1)}, bf16[256,512]{1,0:T(8,128)(2,1)S(1)}, u32[]{:S(2)}, u32[]{:S(2)}) collective-permute-start(bf16[256,512]{1,0:T(8,128)(2,1)} %get-tuple-element.794), channel_id=1, source_target_pairs={{0,4},{4,8},{8,12},{12,16},{16,20},{20,24},{24,28},{28,32},{32,36}... | collective-permute-start | bytes 786440 | tf_op jit(solution)/shard_map/while/body/eval_jaxpr/ppermute | solution.py:21
  64.6 2.7 %collective-permute-start.1 = (bf16[256,64]{0,1:T(8,128)(2,1)S(1)}, bf16[256,64]{0,1:T(8,128)(2,1)S(1)}, u32[]{:S(2)}, u32[]{:S(2)}) collective-permute-start(bf16[256,64]{0,1:T(8,128)(2,1)S(1)} %get-tuple-element.795), channel_id=1, source_target_pairs={{0,4},{4,8},{8,12},{12,16},{16,20},{20,24},{24,28},{28,32},{32,36}... | collective-permute-start | bytes 98312 | tf_op jit(solution)/shard_map/while/body/eval_jaxpr/ppermute | solution.py:21
  69.2 4.4 %collective-permute-start = (bf16[256,512]{1,0:T(8,128)(2,1)}, bf16[256,512]{1,0:T(8,128)(2,1)S(1)}, u32[]{:S(2)}, u32[]{:S(2)}) collective-permute-start(bf16[256,512]{1,0:T(8,128)(2,1)} %get-tuple-element.794), channel_id=1, source_target_pairs={{0,4},{4,8},{8,12},{12,16},{16,20},{20,24},{24,28},{28,32},{32,36}... | collective-permute-start | bytes 786440 | tf_op jit(solution)/shard_map/while/body/eval_jaxpr/ppermute | solution.py:21
  73.6 2.3 %collective-permute-start.1 = (bf16[256,64]{0,1:T(8,128)(2,1)S(1)}, bf16[256,64]{0,1:T(8,128)(2,1)S(1)}, u32[]{:S(2)}, u32[]{:S(2)}) collective-permute-start(bf16[256,64]{0,1:T(8,128)(2,1)S(1)} %get-tuple-element.795), channel_id=1, source_target_pairs={{0,4},{4,8},{8,12},{12,16},{16,20},{20,24},{24,28},{28,32},{32,36}... | collective-permute-start | bytes 98312 | tf_op jit(solution)/shard_map/while/body/eval_jaxpr/ppermute | solution.py:21
  76.6 0.8 collective-permute-done.1
  78.2 7.7 %collective-permute-start = (bf16[256,512]{1,0:T(8,128)(2,1)}, bf16[256,512]{1,0:T(8,128)(2,1)S(1)}, u32[]{:S(2)}, u32[]{:S(2)}) collective-permute-start(bf16[256,512]{1,0:T(8,128)(2,1)} %get-tuple-element.794), channel_id=1, source_target_pairs={{0,4},{4,8},{8,12},{12,16},{16,20},{20,24},{24,28},{28,32},{32,36}... | collective-permute-start | bytes 786440 | tf_op jit(solution)/shard_map/while/body/eval_jaxpr/ppermute | solution.py:21
  85.9 3.0 %collective-permute-start.1 = (bf16[256,64]{0,1:T(8,128)(2,1)S(1)}, bf16[256,64]{0,1:T(8,128)(2,1)S(1)}, u32[]{:S(2)}, u32[]{:S(2)}) collective-permute-start(bf16[256,64]{0,1:T(8,128)(2,1)S(1)} %get-tuple-element.795), channel_id=1, source_target_pairs={{0,4},{4,8},{8,12},{12,16},{16,20},{20,24},{24,28},{28,32},{32,36}... | collective-permute-start | bytes 98312 | tf_op jit(solution)/shard_map/while/body/eval_jaxpr/ppermute | solution.py:21
  90.7 4.2 %collective-permute-start = (bf16[256,512]{1,0:T(8,128)(2,1)}, bf16[256,512]{1,0:T(8,128)(2,1)S(1)}, u32[]{:S(2)}, u32[]{:S(2)}) collective-permute-start(bf16[256,512]{1,0:T(8,128)(2,1)} %get-tuple-element.794), channel_id=1, source_target_pairs={{0,4},{4,8},{8,12},{12,16},{16,20},{20,24},{24,28},{28,32},{32,36}... | collective-permute-start | bytes 786440 | tf_op jit(solution)/shard_map/while/body/eval_jaxpr/ppermute | solution.py:21
  94.9 5.9 %collective-permute-start.1 = (bf16[256,64]{0,1:T(8,128)(2,1)S(1)}, bf16[256,64]{0,1:T(8,128)(2,1)S(1)}, u32[]{:S(2)}, u32[]{:S(2)}) collective-permute-start(bf16[256,64]{0,1:T(8,128)(2,1)S(1)} %get-tuple-element.795), channel_id=1, source_target_pairs={{0,4},{4,8},{8,12},{12,16},{16,20},{20,24},{24,28},{28,32},{32,36}... | collective-permute-start | bytes 98312 | tf_op jit(solution)/shard_map/while/body/eval_jaxpr/ppermute | solution.py:21
  102.6 4.8 %fusion.32 = bf16[256,4096]{1,0:T(8,128)(2,1)} fusion(bf16[4,128,4096]{2,1,0:T(8,128)(2,1)} %bitcast.77, f32[4,256,128]{2,1,0:T(8,128)S(1)} %get-tuple-element.539, f32[4,256]{1,0:T(4,128)S(1)} %get-tuple-element.540), kind=kOutput, calls=%fused_computation.51 | convolution fusion | flops 1075052544 | bytes 6819840 | tf_op jit(solution)/shard_map/hqd,hdm->qm/dot_general | solution.py:146
  107.4 98.2 %all-reduce.2.cloned.1.call-done = bf16[256,4096]{1,0:T(8,128)(2,1)} async-done(((bf16[256,4096]{1,0:T(8,128)(2,1)}), bf16[256,4096]{1,0:T(8,128)(2,1)}) %all-reduce.2.cloned.1.call-update) | async-done | bytes 2097168 | tf_op jit(solution)/shard_map/psum | solution.py:150
  205.7 3.1 %copy.77 = bf16[256,4096]{1,0:T(8,128)(2,1)} copy(bf16[256,4096]{1,0:T(8,128)(2,1)} %all-reduce.2.cloned.1.call-done) | data formatting | bytes 4194304
  (85 shorter events, 14.4 us)
Async XLA Ops:
  6.5 1.5 copy-start
  6.5 6.2 %copy-start.7 = (f32[1024]{0:T(1024)S(1)}, f32[1024]{0:T(1024)}, u32[]{:S(2)}) copy-start(f32[1024]{0:T(1024)} %param.21) | copy-start | bytes 12292
  6.5 9.0 %copy-start.4 = (s32[256]{0:T(256)S(1)}, s32[256]{0:T(256)}, u32[]{:S(2)}) copy-start(s32[256]{0:T(256)} %param.20) | copy-start | bytes 3076
  6.5 8.1 %copy-start.3 = (bf16[256,512]{1,0:T(8,128)(2,1)S(1)}, bf16[256,512]{1,0:T(8,128)(2,1)}, u32[]{:S(2)}) copy-start(bf16[256,512]{1,0:T(8,128)(2,1)} %param.18) | copy-start | bytes 786436
  6.5 6.2 %copy-start.5 = (bf16[256,64]{0,1:T(8,128)(2,1)S(1)}, bf16[256,64]{0,1:T(8,128)(2,1)}, u32[]{:S(2)}) copy-start(bf16[256,64]{0,1:T(8,128)(2,1)} %param.19) | copy-start | bytes 98308
  6.5 8.1 %copy-start.6 = (f32[512]{0:T(512)S(1)}, f32[512]{0:T(512)}, u32[]{:S(2)}) copy-start(f32[512]{0:T(512)} %param.22) | copy-start | bytes 6148
  6.6 9.0 %copy-start.2 = (bf16[512,512]{1,0:T(8,128)(2,1)S(1)}, bf16[512,512]{1,0:T(8,128)(2,1)}, u32[]{:S(2)}) copy-start(bf16[512,512]{1,0:T(8,128)(2,1)} %param.26) | copy-start | bytes 1572868
  6.6 9.0 %copy-start.1 = (bf16[512,512]{1,0:T(8,128)(2,1)S(1)}, bf16[512,512]{1,0:T(8,128)(2,1)}, u32[]{:S(2)}) copy-start(bf16[512,512]{1,0:T(8,128)(2,1)} %param.25) | copy-start | bytes 1572868
  6.6 199.1 %all-reduce.2.cloned.1.call-start = ((), (), s32[]{:S(2)}) async-start(), calls=%async_computation | async-start | bytes 4194304 | tf_op jit(solution)/shard_map/psum | solution.py:150
  22.2 13.8 %collective-permute-start = (bf16[256,512]{1,0:T(8,128)(2,1)}, bf16[256,512]{1,0:T(8,128)(2,1)S(1)}, u32[]{:S(2)}, u32[]{:S(2)}) collective-permute-start(bf16[256,512]{1,0:T(8,128)(2,1)} %get-tuple-element.794), channel_id=1, source_target_pairs={{0,4},{4,8},{8,12},{12,16},{16,20},{20,24},{24,28},{28,32},{32,36}... | collective-permute-start | bytes 786440 | tf_op jit(solution)/shard_map/while/body/eval_jaxpr/ppermute | solution.py:21
  26.8 9.2 %collective-permute-start.1 = (bf16[256,64]{0,1:T(8,128)(2,1)S(1)}, bf16[256,64]{0,1:T(8,128)(2,1)S(1)}, u32[]{:S(2)}, u32[]{:S(2)}) collective-permute-start(bf16[256,64]{0,1:T(8,128)(2,1)S(1)} %get-tuple-element.795), channel_id=1, source_target_pairs={{0,4},{4,8},{8,12},{12,16},{16,20},{20,24},{24,28},{28,32},{32,36}... | collective-permute-start | bytes 98312 | tf_op jit(solution)/shard_map/while/body/eval_jaxpr/ppermute | solution.py:21
  40.7 5.8 %collective-permute-start = (bf16[256,512]{1,0:T(8,128)(2,1)}, bf16[256,512]{1,0:T(8,128)(2,1)S(1)}, u32[]{:S(2)}, u32[]{:S(2)}) collective-permute-start(bf16[256,512]{1,0:T(8,128)(2,1)} %get-tuple-element.794), channel_id=1, source_target_pairs={{0,4},{4,8},{8,12},{12,16},{16,20},{20,24},{24,28},{28,32},{32,36}... | collective-permute-start | bytes 786440 | tf_op jit(solution)/shard_map/while/body/eval_jaxpr/ppermute | solution.py:21
  42.6 3.9 %collective-permute-start.1 = (bf16[256,64]{0,1:T(8,128)(2,1)S(1)}, bf16[256,64]{0,1:T(8,128)(2,1)S(1)}, u32[]{:S(2)}, u32[]{:S(2)}) collective-permute-start(bf16[256,64]{0,1:T(8,128)(2,1)S(1)} %get-tuple-element.795), channel_id=1, source_target_pairs={{0,4},{4,8},{8,12},{12,16},{16,20},{20,24},{24,28},{28,32},{32,36}... | collective-permute-start | bytes 98312 | tf_op jit(solution)/shard_map/while/body/eval_jaxpr/ppermute | solution.py:21
  47.2 12.3 %collective-permute-start = (bf16[256,512]{1,0:T(8,128)(2,1)}, bf16[256,512]{1,0:T(8,128)(2,1)S(1)}, u32[]{:S(2)}, u32[]{:S(2)}) collective-permute-start(bf16[256,512]{1,0:T(8,128)(2,1)} %get-tuple-element.794), channel_id=1, source_target_pairs={{0,4},{4,8},{8,12},{12,16},{16,20},{20,24},{24,28},{28,32},{32,36}... | collective-permute-start | bytes 786440 | tf_op jit(solution)/shard_map/while/body/eval_jaxpr/ppermute | solution.py:21
  55.7 3.9 %collective-permute-start.1 = (bf16[256,64]{0,1:T(8,128)(2,1)S(1)}, bf16[256,64]{0,1:T(8,128)(2,1)S(1)}, u32[]{:S(2)}, u32[]{:S(2)}) collective-permute-start(bf16[256,64]{0,1:T(8,128)(2,1)S(1)} %get-tuple-element.795), channel_id=1, source_target_pairs={{0,4},{4,8},{8,12},{12,16},{16,20},{20,24},{24,28},{28,32},{32,36}... | collective-permute-start | bytes 98312 | tf_op jit(solution)/shard_map/while/body/eval_jaxpr/ppermute | solution.py:21
  60.3 8.2 %collective-permute-start = (bf16[256,512]{1,0:T(8,128)(2,1)}, bf16[256,512]{1,0:T(8,128)(2,1)S(1)}, u32[]{:S(2)}, u32[]{:S(2)}) collective-permute-start(bf16[256,512]{1,0:T(8,128)(2,1)} %get-tuple-element.794), channel_id=1, source_target_pairs={{0,4},{4,8},{8,12},{12,16},{16,20},{20,24},{24,28},{28,32},{32,36}... | collective-permute-start | bytes 786440 | tf_op jit(solution)/shard_map/while/body/eval_jaxpr/ppermute | solution.py:21
  64.6 3.9 %collective-permute-start.1 = (bf16[256,64]{0,1:T(8,128)(2,1)S(1)}, bf16[256,64]{0,1:T(8,128)(2,1)S(1)}, u32[]{:S(2)}, u32[]{:S(2)}) collective-permute-start(bf16[256,64]{0,1:T(8,128)(2,1)S(1)} %get-tuple-element.795), channel_id=1, source_target_pairs={{0,4},{4,8},{8,12},{12,16},{16,20},{20,24},{24,28},{28,32},{32,36}... | collective-permute-start | bytes 98312 | tf_op jit(solution)/shard_map/while/body/eval_jaxpr/ppermute | solution.py:21
  69.2 8.2 %collective-permute-start = (bf16[256,512]{1,0:T(8,128)(2,1)}, bf16[256,512]{1,0:T(8,128)(2,1)S(1)}, u32[]{:S(2)}, u32[]{:S(2)}) collective-permute-start(bf16[256,512]{1,0:T(8,128)(2,1)} %get-tuple-element.794), channel_id=1, source_target_pairs={{0,4},{4,8},{8,12},{12,16},{16,20},{20,24},{24,28},{28,32},{32,36}... | collective-permute-start | bytes 786440 | tf_op jit(solution)/shard_map/while/body/eval_jaxpr/ppermute | solution.py:21
  73.6 3.9 %collective-permute-start.1 = (bf16[256,64]{0,1:T(8,128)(2,1)S(1)}, bf16[256,64]{0,1:T(8,128)(2,1)S(1)}, u32[]{:S(2)}, u32[]{:S(2)}) collective-permute-start(bf16[256,64]{0,1:T(8,128)(2,1)S(1)} %get-tuple-element.795), channel_id=1, source_target_pairs={{0,4},{4,8},{8,12},{12,16},{16,20},{20,24},{24,28},{28,32},{32,36}... | collective-permute-start | bytes 98312 | tf_op jit(solution)/shard_map/while/body/eval_jaxpr/ppermute | solution.py:21
  78.2 11.8 %collective-permute-start = (bf16[256,512]{1,0:T(8,128)(2,1)}, bf16[256,512]{1,0:T(8,128)(2,1)S(1)}, u32[]{:S(2)}, u32[]{:S(2)}) collective-permute-start(bf16[256,512]{1,0:T(8,128)(2,1)} %get-tuple-element.794), channel_id=1, source_target_pairs={{0,4},{4,8},{8,12},{12,16},{16,20},{20,24},{24,28},{28,32},{32,36}... | collective-permute-start | bytes 786440 | tf_op jit(solution)/shard_map/while/body/eval_jaxpr/ppermute | solution.py:21
  85.9 4.0 %collective-permute-start.1 = (bf16[256,64]{0,1:T(8,128)(2,1)S(1)}, bf16[256,64]{0,1:T(8,128)(2,1)S(1)}, u32[]{:S(2)}, u32[]{:S(2)}) collective-permute-start(bf16[256,64]{0,1:T(8,128)(2,1)S(1)} %get-tuple-element.795), channel_id=1, source_target_pairs={{0,4},{4,8},{8,12},{12,16},{16,20},{20,24},{24,28},{28,32},{32,36}... | collective-permute-start | bytes 98312 | tf_op jit(solution)/shard_map/while/body/eval_jaxpr/ppermute | solution.py:21
  90.7 11.1 %collective-permute-start = (bf16[256,512]{1,0:T(8,128)(2,1)}, bf16[256,512]{1,0:T(8,128)(2,1)S(1)}, u32[]{:S(2)}, u32[]{:S(2)}) collective-permute-start(bf16[256,512]{1,0:T(8,128)(2,1)} %get-tuple-element.794), channel_id=1, source_target_pairs={{0,4},{4,8},{8,12},{12,16},{16,20},{20,24},{24,28},{28,32},{32,36}... | collective-permute-start | bytes 786440 | tf_op jit(solution)/shard_map/while/body/eval_jaxpr/ppermute | solution.py:21
  94.9 6.9 %collective-permute-start.1 = (bf16[256,64]{0,1:T(8,128)(2,1)S(1)}, bf16[256,64]{0,1:T(8,128)(2,1)S(1)}, u32[]{:S(2)}, u32[]{:S(2)}) collective-permute-start(bf16[256,64]{0,1:T(8,128)(2,1)S(1)} %get-tuple-element.795), channel_id=1, source_target_pairs={{0,4},{4,8},{8,12},{12,16},{16,20},{20,24},{24,28},{28,32},{32,36}... | collective-permute-start | bytes 98312 | tf_op jit(solution)/shard_map/while/body/eval_jaxpr/ppermute | solution.py:21
Sparse Core Ops, SparseCore 0:
  107.5 98.0 all-reduce.1
where the time goes:
time: 217 us; the launch traced here: 216 us
  waiting for transfers between devices  109 us (50%)
  starting transfers between devices  55.3 us (25%)
  between operations  14.3 us (7%)
  matrix products  14 us (6%)
  local copies, waits for them, and re-layouts  10.1 us (5%)
  other arithmetic  7.5 us (3%)
  loops' own time  5.3 us (2%)
    psum x1, waiting for transfers between devices, on_device(): mixed = lax.psum(group_term.astype(jnp.bfloat16), 'tp')  98.2 us
    ppermute x14, starting transfers between devices, from_behind(): lax.ppermute(value, axis, [(source, source + steps) for source in range(i...  55.3 us
    ppermute x14, waiting for transfers between devices, from_behind(): lax.ppermute(value, axis, [(source, source + steps) for source in range(i...  10.9 us
    another operation x1, loops' own time, on_device(): lax.fori_loop(0, SPAN - 1, advance, (payload, softmax_state))  5.06 us
    while x14, local copies, waits for them, and re-layouts  4.96 us
    dot_general x1, matrix products, on_device(): jnp.einsum('hqd,hdm->qm', attended, weight_heads, preferred_element_type=...  4.84 us
  transfers between devices with their start and end apart: 15, of which 8 were waited for; matrix products, arithmetic and copies ran while one was open for 0% of the time, Pallas kernels for 0%

commit v1 on v0

v1 whole, which is shorter than its diff:
```python
import functools

import jax
import jax.numpy as jnp
from jax import lax
from jax.experimental import pallas as pl
from jax.experimental.pallas import tpu as pltpu
from jax.sharding import PartitionSpec as P

MESH = pl.DeviceIdType.MESH
CONTENT = 128
ROTARY = 64
SPAN = 8
NORM_EPS = 1e-06
THETA = 10000.0
MASKED = -1e30
LOG2E = 1.4426950408889634
F32 = jnp.float32
BF16 = jnp.bfloat16
WHOLE = pl.BlockSpec(memory_space=pltpu.VMEM)


def copy_to(src, dst, send, recv, sp, tp):
    return pltpu.make_async_remote_copy(
        src_ref=src,
        dst_ref=dst,
        send_sem=send,
        recv_sem=recv,
        device_id={"sp": sp, "tp": tp},
        device_id_type=MESH,
    )


def rms_scale(entries, gain):
    entries = entries.astype(F32)
    mean = jnp.mean(entries * entries, axis=-1, keepdims=True)
    return (entries * lax.rsqrt(mean + NORM_EPS) * gain).astype(BF16)


def rotate(entries, cosine, sine):
    width = entries.shape[-1]
    lane = lax.broadcasted_iota(jnp.int32, entries.shape, 1)
    ahead = pltpu.roll(entries, width - ROTARY // 2, 1)
    behind = pltpu.roll(entries, ROTARY // 2, 1)
    other = jnp.where(lane % ROTARY < ROTARY // 2, ahead, behind)
    return entries * cosine + other * sine


def payload_kernel(shared_ref, rotary_ref, cos_ref, sin_ref, gain_ref, out_ref):
    rank = shared_ref.shape[1]
    out_ref[:, :rank] = rms_scale(shared_ref[...], gain_ref[...])
    turned = rotate(rotary_ref[...].astype(F32), cos_ref[...], sin_ref[...])
    out_ref[:, rank:] = turned.astype(BF16)


def exchange_kernel(
    pay_ref, win_ref, own_sem, y_send, y_recv, x_send, x_recv, d_send, d_recv
):
    count = lax.axis_size("sp")
    ring = lax.axis_size("tp")
    me = lax.axis_index("sp")
    col = lax.axis_index("tp")
    core = lax.rem(me, 2)
    sibling = me + 1 - 2 * core
    east = lax.rem(col + 1, ring)
    west = lax.rem(col + ring - 1, ring)
    length = pay_ref.shape[0]
    quarter = length // 4
    eighth = length // 8

    def chip_on(steps):
        return lax.rem(me + 2 * steps + count, count)

    def rows(owner, offset, size):
        return pl.ds(pl.multiple_of(owner * quarter + offset, eighth), size)

    far_to = lax.rem(me + 7, count)
    far_from = lax.rem(me - 7 + count, count)
    barrier = pltpu.get_barrier_semaphore()
    for steps in (1, 2, 3):
        pl.semaphore_signal(
            barrier, inc=1, device_id={"sp": chip_on(-steps), "tp": col}, device_id_type=MESH
        )
    for to in (east, west):
        pl.semaphore_signal(barrier, inc=1, device_id={"sp": me, "tp": to}, device_id_type=MESH)
    pl.semaphore_signal(
        barrier, inc=1, device_id={"sp": sibling, "tp": col}, device_id_type=MESH
    )

    @pl.when(core == 0)
    def _():
        pl.semaphore_signal(
            barrier, inc=1, device_id={"sp": far_from, "tp": col}, device_id_type=MESH
        )
        pl.semaphore_wait(barrier, 6)

    @pl.when(core == 1)
    def _():
        pl.semaphore_wait(barrier, 7)

    def y_copy(steps):
        part = rows(col, 0, quarter)
        return copy_to(
            pay_ref.at[part],
            win_ref.at[2 * steps, part],
            y_send.at[steps],
            y_recv.at[steps],
            chip_on(steps),
            col,
        )

    def far_copy():
        part = rows(col, 0, quarter)
        return copy_to(
            pay_ref.at[part], win_ref.at[7, part], y_send.at[4], y_recv.at[4], far_to, col
        )

    def x_copy(lane, slot, kind):
        if kind == 0:
            part, to = rows(col, 0, quarter), east
        elif kind == 1:
            part, to = rows(col, 0, quarter), west
        elif kind == 2:
            part, to = rows(west, 0, eighth), east
        else:
            part, to = rows(east, eighth, eighth), west
        return copy_to(
            win_ref.at[slot, part],
            win_ref.at[slot, part],
            x_send.at[lane, kind],
            x_recv.at[lane, kind],
            me,
            to,
        )

    def d_copy(index, src, slot):
        return copy_to(
            src, win_ref.at[slot], d_send.at[index], d_recv.at[index], sibling, col
        )

    own = pltpu.make_async_copy(pay_ref, win_ref.at[0], own_sem)
    own.start()
    for steps in (1, 2, 3):
        y_copy(steps).start()

    @pl.when(core == 1)
    def _():
        far_copy().start()

    @pl.when(core == 0)
    def _():
        d_copy(0, pay_ref, 1).start()

    def spread(lane, slot):
        x_copy(lane, slot, 0).start()
        x_copy(lane, slot, 1).start()

    def relay(lane, slot):
        x_copy(lane, slot, 0).wait_recv()
        x_copy(lane, slot, 2).start()
        x_copy(lane, slot, 1).wait_recv()
        x_copy(lane, slot, 3).start()

    def finish(lane, slot):
        x_copy(lane, slot, 2).wait_recv()
        x_copy(lane, slot, 3).wait_recv()

    def to_sibling(steps):
        @pl.when(core == 0)
        def _():
            d_copy(steps, win_ref.at[2 * steps], 2 * steps + 1).start()

        @pl.when(core == 1)
        def _():
            d_copy(steps, win_ref.at[2 * steps], 2 * steps - 1).start()

    y_copy(1).wait_recv()
    spread(1, 2)
    y_copy(2).wait_recv()
    spread(2, 4)
    relay(1, 2)
    y_copy(3).wait_recv()
    spread(3, 6)
    finish(1, 2)
    to_sibling(1)
    relay(2, 4)

    @pl.when(core == 0)
    def _():
        far_copy().wait_recv()
        spread(4, 7)

    finish(2, 4)
    to_sibling(2)
    relay(3, 6)

    @pl.when(core == 0)
    def _():
        relay(4, 7)

    finish(3, 6)
    to_sibling(3)

    @pl.when(core == 0)
    def _():
        finish(4, 7)

    own.wait()
    for steps in (1, 2, 3):
        y_copy(steps).wait_send()
        for kind in range(4):
            x_copy(steps, 2 * steps, kind).wait_send()

    @pl.when(core == 0)
    def _():
        d_copy(0, pay_ref, 1).wait_send()
        for steps in (1, 2, 3):
            d_copy(steps, win_ref.at[2 * steps], 2 * steps + 1).wait_send()
            d_copy(steps, win_ref.at[2 * steps], 2 * steps - 1).wait_recv()
        for kind in range(4):
            x_copy(4, 7, kind).wait_send()

    @pl.when(core == 1)
    def _():
        far_copy().wait_send()
        d_copy(0, pay_ref, 1).wait_recv()
        for steps in (1, 2, 3):
            d_copy(steps, win_ref.at[2 * steps], 2 * steps - 1).wait_send()
            d_copy(steps, win_ref.at[2 * steps], 2 * steps + 1).wait_recv()


def attention_kernel(
    latent_ref,
    start_ref,
    win_ref,
    cos_ref,
    sin_ref,
    gain_ref,
    content_ref,
    rotary_ref,
    key_ref,
    value_ref,
    out_ref,
    query,
    highest,
    denominator,
    summed,
):
    length, rank = latent_ref.shape[0], key_ref.shape[0]
    heads = key_ref.shape[1] // CONTENT
    anchor = lax.axis_index("sp") * length
    scale = (CONTENT + ROTARY) ** (-0.5) * LOG2E
    normed = rms_scale(latent_ref[...], gain_ref[...])
    content = jnp.dot(normed, content_ref[...], preferred_element_type=F32).astype(BF16)
    raw = jnp.dot(normed, rotary_ref[...], preferred_element_type=F32)
    lane = lax.broadcasted_iota(jnp.int32, (length, 2 * ROTARY), 1)
    for head in range(heads):
        pair = raw[:, (head // 2) * 2 * ROTARY : (head // 2 + 1) * 2 * ROTARY]
        turned = rotate(pair, cos_ref[...], sin_ref[...])
        turned = jnp.where(lane // ROTARY == head % 2, turned, 0.0).astype(BF16)
        query[head, :, :CONTENT] = content[:, head * CONTENT : (head + 1) * CONTENT]
        query[head, :, CONTENT:] = turned
    highest[...] = jnp.full(highest.shape, MASKED, F32)
    denominator[...] = jnp.zeros(denominator.shape, F32)
    summed[...] = jnp.zeros(summed.shape, F32)
    starts = start_ref[...]
    places = anchor + lax.broadcasted_iota(jnp.int32, (length, 1), 0)

    def absorb(slot, carry):
        shared = win_ref[slot, :, :rank]
        turn = win_ref[slot, :, rank:]
        keys = jnp.dot(shared, key_ref[...], preferred_element_type=F32).astype(BF16)
        values = jnp.dot(shared, value_ref[...], preferred_element_type=F32).astype(BF16)
        key_places = (
            anchor - slot * length + lax.broadcasted_iota(jnp.int32, (length, length), 1)
        )
        visible = (key_places >= starts) & (key_places <= places)
        for head in range(heads):
            cut = slice(head * CONTENT, (head + 1) * CONTENT)
            joined = jnp.concatenate([keys[:, cut], turn], axis=1)
            scores = lax.dot_general(
                query[head], joined, (((1,), (1,)), ((), ())), preferred_element_type=F32
            )
            scores = jnp.where(visible, scores * scale, MASKED)
            before = highest[head]
            after = jnp.maximum(before, jnp.max(scores, axis=-1, keepdims=True))
            factor = jnp.exp2(before - after)
            weights = jnp.exp2(scores - after)
            highest[head] = after
            denominator[head] = denominator[head] * factor + jnp.sum(
                weights, axis=-1, keepdims=True
            )
            summed[head] = summed[head] * factor + jnp.dot(
                weights.astype(BF16), values[:, cut], preferred_element_type=F32
            )
        return carry

    lax.fori_loop(0, SPAN, absorb, 0)
    for head in range(heads):
        cut = slice(head * CONTENT, (head + 1) * CONTENT)
        out_ref[:, cut] = (summed[head] / denominator[head]).astype(BF16)


CHUNKS = 4


def output_kernel(
    attended_ref, weight_ref, out_ref, term, first, second, held, sums, send, recv
):
    col = lax.axis_index("tp")
    me = lax.axis_index("sp")
    ring = lax.axis_size("tp")
    length, model = out_ref.shape
    size = length // CHUNKS
    half, piece = model // 4, model // 8
    bit = col // 2
    gray = lax.rem(col + bit, 2)
    near = (col + 1 - 2 * lax.rem(col, 2), ring - 1 - col)
    keep = (gray, bit)
    sub = (bit, gray)

    barrier = pltpu.get_barrier_semaphore()
    for partner in near:
        pl.semaphore_signal(
            barrier, inc=1, device_id={"sp": me, "tp": partner}, device_id_type=MESH
        )
    pl.semaphore_wait(barrier, 2)

    def rows(chunk):
        return pl.ds(chunk * size, size)

    def half_at(side, which):
        return pl.multiple_of(side * (model // 2) + which * half, half)

    def piece_at(side, which, sub_which):
        return pl.multiple_of(side * (model // 2) + which * half + sub_which * piece, piece)

    def copy(kind, side, chunk, src, dst, partner):
        return copy_to(
            src, dst, send.at[kind, side, chunk], recv.at[kind, side, chunk], me, partner
        )

    def stage_one(side, chunk):
        return copy(
            0,
            side,
            chunk,
            term.at[rows(chunk), pl.ds(half_at(side, 1 - keep[side]), half)],
            first.at[side, rows(chunk)],
            near[side],
        )

    def stage_two(side, chunk):
        return copy(
            1,
            side,
            chunk,
            held.at[side, rows(chunk)],
            second.at[side, rows(chunk)],
            near[1 - side],
        )

    def own_piece(side, chunk):
        return out_ref.at[rows(chunk), pl.ds(piece_at(side, keep[side], sub[side]), piece)]

    def gather(kind, side, chunk):
        if kind == 4:
            ref = out_ref.at[
                rows(chunk), pl.ds(piece_at(side, keep[side], 1 - sub[side]), piece)
            ]
        else:
            ref = own_piece(side, chunk)
        return copy(kind, side, chunk, ref, ref, near[1 - side] if kind == 2 else near[side])

    for chunk in range(CHUNKS):
        mine = attended_ref[rows(chunk), :]
        for block in range(model // half):
            cut = pl.ds(block * half, half)
            term[rows(chunk), cut] = jnp.dot(
                mine, weight_ref[:, cut], preferred_element_type=F32
            ).astype(BF16)
        for side in (0, 1):
            stage_one(side, chunk).start()

    for chunk in range(CHUNKS):
        for side in (0, 1):
            stage_one(side, chunk).wait_recv()
            base = half_at(side, keep[side])
            theirs = pl.multiple_of((1 - sub[side]) * piece, piece)
            ours = pl.multiple_of(sub[side] * piece, piece)
            held[side, rows(chunk), :] = (
                term[rows(chunk), pl.ds(pl.multiple_of(base + theirs, piece), piece)].astype(F32)
                + first[side, rows(chunk), pl.ds(theirs, piece)].astype(F32)
            ).astype(BF16)
            stage_two(side, chunk).start()
            sums[side, rows(chunk), :] = term[
                rows(chunk), pl.ds(pl.multiple_of(base + ours, piece), piece)
            ].astype(F32) + first[side, rows(chunk), pl.ds(ours, piece)].astype(F32)

    for chunk in range(CHUNKS):
        for side in (0, 1):
            stage_two(side, chunk).wait_recv()
            cut = pl.ds(piece_at(side, keep[side], sub[side]), piece)
            out_ref[rows(chunk), cut] = (
                sums[side, rows(chunk), :] + second[side, rows(chunk), :].astype(F32)
            ).astype(BF16)
            gather(2, side, chunk).start()
            gather(3, side, chunk).start()

    for chunk in range(CHUNKS):
        for side in (0, 1):
            gather(2, side, chunk).wait_recv()
            gather(4, side, chunk).start()

    for chunk in range(CHUNKS):
        for side in (0, 1):
            gather(3, side, chunk).wait_recv()
            gather(4, side, chunk).wait_recv()
            stage_one(side, chunk).wait_send()
            stage_two(side, chunk).wait_send()
            for kind in (2, 3, 4):
                gather(kind, side, chunk).wait_send()


def on_device(
    query_latent,
    shared_latent,
    rotary_key,
    document_start,
    query_gain,
    shared_gain,
    content_weight,
    rotary_weight,
    key_weight,
    value_weight,
    output_weight,
):
    length = query_latent.shape[0]
    rank = shared_latent.shape[1]
    model = output_weight.shape[1]
    heads = key_weight.shape[1] // CONTENT
    width = rank + 2 * ROTARY
    places = lax.axis_index("sp") * length + jnp.arange(length, dtype=jnp.int32)
    frequency = 1.0 / THETA ** (jnp.arange(0, ROTARY, 2, dtype=F32) / ROTARY)
    angles = places.astype(F32)[:, None] * frequency[None, :]
    cosine, sine = jnp.cos(angles), jnp.sin(angles)
    cosine = jnp.concatenate([cosine] * 4, axis=1)
    sine = jnp.concatenate([-sine, sine, -sine, sine], axis=1)
    rotary_pair = jnp.concatenate([rotary_key, rotary_key], axis=1)
    payload = pl.pallas_call(
        payload_kernel,
        out_shape=jax.ShapeDtypeStruct((length, width), BF16),
        in_specs=[WHOLE] * 5,
        out_specs=WHOLE,
        name="payload",
    )(shared_latent, rotary_pair, cosine, sine, shared_gain[None, :])
    window = pl.pallas_call(
        exchange_kernel,
        out_shape=jax.ShapeDtypeStruct((SPAN, length, width), BF16),
        in_specs=[WHOLE],
        out_specs=WHOLE,
        scratch_shapes=[
            pltpu.SemaphoreType.DMA,
            pltpu.SemaphoreType.DMA((5,)),
            pltpu.SemaphoreType.DMA((5,)),
            pltpu.SemaphoreType.DMA((5, 4)),
            pltpu.SemaphoreType.DMA((5, 4)),
            pltpu.SemaphoreType.DMA((4,)),
            pltpu.SemaphoreType.DMA((4,)),
        ],
        compiler_params=pltpu.CompilerParams(collective_id=0, has_side_effects=True),
        name="exchange",
    )(payload)
    attended = pl.pallas_call(
        attention_kernel,
        out_shape=jax.ShapeDtypeStruct((length, heads * CONTENT), BF16),
        in_specs=[WHOLE] * 10,
        out_specs=WHOLE,
        scratch_shapes=[
            pltpu.VMEM((heads, length, 2 * CONTENT), BF16),
            pltpu.VMEM((heads, length, 1), F32),
            pltpu.VMEM((heads, length, 1), F32),
            pltpu.VMEM((heads, length, CONTENT), F32),
        ],
        name="attention",
    )(
        query_latent,
        document_start[:, None],
        window,
        cosine,
        sine,
        query_gain[None, :],
        content_weight,
        rotary_weight,
        key_weight,
        value_weight,
    )
    mixed = pl.pallas_call(
        output_kernel,
        out_shape=jax.ShapeDtypeStruct((length, model), BF16),
        in_specs=[WHOLE] * 2,
        out_specs=WHOLE,
        scratch_shapes=[
            pltpu.VMEM((length, model), BF16),
            pltpu.VMEM((2, length, model // 4), BF16),
            pltpu.VMEM((2, length, model // 8), BF16),
            pltpu.VMEM((2, length, model // 8), BF16),
            pltpu.VMEM((2, length, model // 8), F32),
            pltpu.SemaphoreType.DMA((5, 2, CHUNKS)),
            pltpu.SemaphoreType.DMA((5, 2, CHUNKS)),
        ],
        compiler_params=pltpu.CompilerParams(collective_id=1, has_side_effects=True),
        name="output",
    )(attended, output_weight)
    return mixed


def solution(mesh):
    return jax.shard_map(
        on_device,
        mesh=mesh,
        in_specs=(
            P("sp", None),
            P("sp", None),
            P("sp", None),
            P("sp"),
            P(),
            P(),
            P(None, "tp"),
            P(None, "tp"),
            P(None, "tp"),
            P(None, "tp"),
            P("tp", None),
        ),
        out_specs=P("sp", None),
        check_vma=False,
    )
```

time: 217 us -> 126 us (0.58)
  Pallas kernels: 0 us -> 118 us
  waiting for transfers between devices: 109 us -> 0 us
  starting transfers between devices: 55.3 us -> 0 us
  between operations: 14.3 us -> 0.03 us
  matrix products: 14 us -> 0 us
  loops' own time: 5.3 us -> 0 us
  other arithmetic: 7.5 us -> 2.24 us
  local copies, waits for them, and re-layouts: 10.1 us -> 5.46 us
    pallas_call x0 -> x4, Pallas kernels: none -> 118 us  [the longest x1 45 us: on_device(): pl.pallas_call(exchange_kernel, out_shape=jax.ShapeDtypeStruct((SPAN, len...]
    psum x1 -> x0, waiting for transfers between devices: 98.2 us -> none  [on_device(): mixed = lax.psum(group_term.astype(jnp.bfloat16), 'tp')]
    ppermute x14 -> x0, starting transfers between devices: 55.3 us -> none  [from_behind(): lax.ppermute(value, axis, [(source, source + steps) for source in range(i...]
    dot_general x13 -> x0, matrix products: 14 us -> none  [the longest x1 4.84 us: on_device(): jnp.einsum('hqd,hdm->qm', attended, weight_heads, preferred_element_type=...]
    ppermute x14 -> x0, waiting for transfers between devices: 10.9 us -> none  [from_behind(): lax.ppermute(value, axis, [(source, source + steps) for source in range(i...]
    another operation x9 -> x0, loops' own time: 5.3 us -> none  [the longest x1 5.06 us: on_device(): lax.fori_loop(0, SPAN - 1, advance, (payload, softmax_state))]
    while x14 -> x0, local copies, waits for them, and re-layouts: 4.96 us -> none
    reduce_sum x4 -> x0, other arithmetic: 3.45 us -> none  [the longest x2 2.45 us: rms_scale(): jnp.mean(entries * entries, axis=-1, keepdims=True) + norm_eps]
  transfers between devices with their start and end apart: 15 -> 0, of which waited for: 8 -> 0; matrix products, arithmetic and copies ran while one was open for 0% -> 0% of each run, Pallas kernels for 0% -> 0%
where the time goes in v1:
time: 126 us
  Pallas kernels  118 us (94%)
  local copies, waits for them, and re-layouts  5.46 us (4%)
  other arithmetic  2.24 us (2%)
    pallas_call x1, Pallas kernels, on_device(): pl.pallas_call(exchange_kernel, out_shape=jax.ShapeDtypeStruct((SPAN, len...  45 us
    pallas_call x1, Pallas kernels, on_device(): pl.pallas_call(output_kernel, out_shape=jax.ShapeDtypeStruct((length, mod...  42.9 us
    pallas_call x1, Pallas kernels, on_device(): pl.pallas_call(attention_kernel, out_shape=jax.ShapeDtypeStruct((length,...  28.2 us
    unnamed x2, local copies, waits for them, and re-layouts  4 us

profile of v1, /device:TPU:1, one launch (start us, length us, event | category | flops | bytes accessed | tf_op | source)
XLA Modules:
  0.0 125.8 jit_solution(3090692574821021386)
XLA Ops:
  0.0 0.9 copy.17
  0.9 0.7 pad_maximum_fusion.2.rotary_ref
  1.6 1.5 %copy.20.start_ref = s32[256,1]{1,0:T(8,128)} copy(s32[256,1]{0,1:T(1,128)} %bitcast.5) | data formatting | bytes 2048 | tf_op jit(solution)/shard_map/broadcast_in_dim | solution.py:488
  3.1 0.5 fusion
  3.6 1.0 pad_maximum_fusion
  4.6 2.0 %payload.1.pay_ref = bf16[256,640]{1,0:T(8,128)(2,1)} custom-call(bf16[256,512]{1,0:T(8,128)(2,1)} %shared_ref.1, bf16[256,128]{1,0:T(8,128)(2,1)} %pad_maximum_fusion.2.rotary_ref, f32[256,128]{1,0:T(8,128)} %get-tuple-element.8.cos_ref, f32[256,128]{1,0:T(8,128)} %get-tuple-element.9.sin_ref, f32[1,512]{1,0:T(1,128)} %bitcast.4), custom_call_target="tpu_custom_call" | custom-call | tf_op jit(solution)/shard_map/payload/pallas_call | solution.py:450
  6.6 45.0 %exchange.1.win_ref = bf16[8,256,640]{2,1,0:T(8,128)(2,1)} custom-call(bf16[256,640]{1,0:T(8,128)(2,1)} %payload.1.pay_ref), custom_call_target="tpu_custom_call" | custom-call | tf_op jit(solution)/shard_map/exchange/pallas_call | solution.py:457
  51.5 28.2 %attention.1.attended_ref = bf16[256,512]{1,0:T(8,128)(2,1)} custom-call(bf16[256,1024]{1,0:T(8,128)(2,1)} %latent_ref.1, s32[256,1]{1,0:T(8,128)} %copy.20.start_ref, bf16[8,256,640]{2,1,0:T(8,128)(2,1)} %exchange.1.win_ref, f32[256,128]{1,0:T(8,128)} %get-tuple-element.8.cos_ref, f32[256,128]{1,0:T(8,128)} %get-tuple-element.9.sin_ref, f32[1,1024]{1,0:T(1,128)} %bitcast.3, ...), custom_call_target="tpu_custom_call" | custom-call | tf_op jit(solution)/shard_map/attention/pallas_call | solution.py:474
  79.8 42.9 %output.1 = bf16[256,4096]{1,0:T(8,128)(2,1)} custom-call(bf16[256,512]{1,0:T(8,128)(2,1)} %attention.1.attended_ref, bf16[512,4096]{1,0:T(8,128)(2,1)} %weight_ref.1), custom_call_target="tpu_custom_call" | custom-call | tf_op jit(solution)/shard_map/output/pallas_call | solution.py:498
  122.7 3.1 %copy.22 = bf16[256,4096]{1,0:T(8,128)(2,1)} copy(bf16[256,4096]{1,0:T(8,128)(2,1)} %output.1) | data formatting | bytes 4194304
  (2 shorter events, 0.0 us)

commit v2 on v0

v2 whole, which is shorter than its diff:
```python
import jax
import jax.numpy as jnp
from jax import lax
from jax.experimental import pallas as pl
from jax.experimental.pallas import tpu as pltpu
from jax.sharding import PartitionSpec as P

MESH = pl.DeviceIdType.MESH
CONTENT = 128
ROTARY = 64
SPAN = 8
NORM_EPS = 1e-06
THETA = 10000.0
MASKED = -1e30
LOG2E = 1.4426950408889634
F32 = jnp.float32
BF16 = jnp.bfloat16
WHOLE = pl.BlockSpec(memory_space=pltpu.VMEM)
FAR = pl.BlockSpec(memory_space=pltpu.HBM)
CHUNKS = 4


def copy_to(src, dst, send, recv, sp, tp):
    return pltpu.make_async_remote_copy(
        src_ref=src,
        dst_ref=dst,
        send_sem=send,
        recv_sem=recv,
        device_id={"sp": sp, "tp": tp},
        device_id_type=MESH,
    )


def rms_scale(entries, gain):
    entries = entries.astype(F32)
    mean = jnp.mean(entries * entries, axis=-1, keepdims=True)
    return (entries * lax.rsqrt(mean + NORM_EPS) * gain).astype(BF16)


def rotate(entries, cosine, sine):
    width = entries.shape[-1]
    lane = lax.broadcasted_iota(jnp.int32, entries.shape, 1)
    ahead = pltpu.roll(entries, width - ROTARY // 2, 1)
    behind = pltpu.roll(entries, ROTARY // 2, 1)
    other = jnp.where(lane % ROTARY < ROTARY // 2, ahead, behind)
    return entries * cosine + other * sine


def mixed_kernel(
    latent_hbm,
    shared_ref,
    rotary_ref,
    start_ref,
    cos_ref,
    sin_ref,
    query_gain_ref,
    shared_gain_ref,
    content_hbm,
    rotary_weight_hbm,
    key_hbm,
    value_hbm,
    output_hbm,
    out_ref,
    latent_ref,
    content_ref,
    rotary_weight_ref,
    key_ref,
    value_ref,
    weight_ref,
    value_turned,
    pay_ref,
    win_ref,
    query,
    highest,
    denominator,
    summed,
    attended,
    term,
    first,
    second,
    held,
    load_sem,
    y_send,
    y_recv,
    x_send,
    x_recv,
    d_send,
    d_recv,
    send,
    recv,
):
    count, ring = lax.axis_size("sp"), lax.axis_size("tp")
    me, col = lax.axis_index("sp"), lax.axis_index("tp")
    core = lax.rem(me, 2)
    chip, chips = me // 2, count // 2
    sibling = me + 1 - 2 * core
    east, west = lax.rem(col + 1, ring), lax.rem(col + ring - 1, ring)
    length, rank = shared_ref.shape
    heads = key_ref.shape[1] // CONTENT
    model = out_ref.shape[1]
    quarter, eighth = length // 4, length // 8

    def load(index, src, dst):
        return pltpu.make_async_copy(src, dst, load_sem.at[index])

    loads = [
        load(0, latent_hbm, latent_ref),
        load(1, content_hbm, content_ref),
        load(2, rotary_weight_hbm, rotary_weight_ref),
        load(3, value_hbm, value_ref),
        load(4, key_hbm, key_ref),
        load(5, output_hbm, weight_ref),
    ]
    for item in loads:
        item.start()

    barrier = pltpu.get_barrier_semaphore()

    def greet(sp, tp):
        pl.semaphore_signal(barrier, inc=1, device_id={"sp": sp, "tp": tp}, device_id_type=MESH)

    def has(steps):
        return chip >= steps

    def feeds(steps):
        return chip + steps < chips

    greet(me, east)
    greet(me, west)
    greet(sibling, col)
    for steps in (1, 2, 3):

        @pl.when(has(steps))
        def _():
            greet(me - 2 * steps, col)

    @pl.when((core == 0) & has(4))
    def _():
        greet(me - 7, col)

    pay_ref[:, :rank] = rms_scale(shared_ref[...], shared_gain_ref[...])
    leading = rotary_ref[: ROTARY // 2, :].astype(F32)
    trailing = rotary_ref[ROTARY // 2 :, :].astype(F32)
    cosine, sine = cos_ref[...], sin_ref[...]
    turned = [leading * cosine - trailing * sine, leading * sine + trailing * cosine]
    pay_ref[:, rank:] = jnp.concatenate(turned * 2, axis=0).T.astype(BF16)

    def rows(owner, offset, size):
        return pl.ds(pl.multiple_of(owner * quarter + offset, eighth), size)

    def y_copy(steps):
        part = rows(col, 0, quarter)
        slot, to = (2 * steps, me + 2 * steps) if steps < 4 else (7, me + 7)
        return copy_to(
            pay_ref.at[part], win_ref.at[slot, part], y_send.at[steps], y_recv.at[steps], to, col
        )

    def x_copy(lane, kind):
        slot = 2 * lane if lane < 4 else 7
        if kind == 0:
            part, to = rows(col, 0, quarter), east
        elif kind == 1:
            part, to = rows(col, 0, quarter), west
        elif kind == 2:
            part, to = rows(west, 0, eighth), east
        else:
            part, to = rows(east, eighth, eighth), west
        ref = win_ref.at[slot, part]
        return copy_to(ref, ref, x_send.at[lane, kind], x_recv.at[lane, kind], me, to)

    def d_copy(lane, shift):
        src = win_ref.at[2 * lane] if lane else pay_ref
        return copy_to(
            src, win_ref.at[2 * lane + shift], d_send.at[lane], d_recv.at[lane], sibling, col
        )

    def on_core(which, also=None):
        mine = core == which
        return pl.when(mine if also is None else mine & also)

    far = (core == 1) & feeds(4)
    number = 3 + jnp.minimum(3, chips - 1 - chip) + far.astype(jnp.int32)
    pl.semaphore_wait(barrier, number)
    for steps in (1, 2, 3):

        @pl.when(feeds(steps))
        def _():
            y_copy(steps).start()

    @pl.when(far)
    def _():
        y_copy(4).start()

    @on_core(0)
    def _():
        d_copy(0, 1).start()

    def arrived(lane):
        y_copy(lane).wait_recv()
        x_copy(lane, 0).start()
        x_copy(lane, 1).start()

    def relay(lane):
        x_copy(lane, 0).wait_recv()
        x_copy(lane, 2).start()
        x_copy(lane, 1).wait_recv()
        x_copy(lane, 3).start()

    def finish(lane):
        x_copy(lane, 2).wait_recv()
        x_copy(lane, 3).wait_recv()
        if lane < 4:

            @on_core(0)
            def _():
                d_copy(lane, 1).start()

            @on_core(1)
            def _():
                d_copy(lane, -1).start()

    def from_sibling(lane):
        @on_core(0)
        def _():
            d_copy(lane, -1).wait_recv()

        @on_core(1)
        def _():
            d_copy(lane, 1).wait_recv()

    scale = (CONTENT + ROTARY) ** (-0.5) * LOG2E
    for item in loads[:3]:
        item.wait()
    normed = rms_scale(latent_ref[...], query_gain_ref[...])
    content = jnp.dot(normed, content_ref[...], preferred_element_type=F32).astype(BF16)
    raw = jnp.dot(normed, rotary_weight_ref[...], preferred_element_type=F32)
    wide_cosine = jnp.concatenate([cosine] * 4, axis=0).T
    wide_sine = jnp.concatenate([-sine, sine, -sine, sine], axis=0).T
    lane_of = lax.broadcasted_iota(jnp.int32, (length, 2 * ROTARY), 1)
    for head in range(heads):
        cut = slice(head // 2 * 2 * ROTARY, (head // 2 + 1) * 2 * ROTARY)
        pair = rotate(raw[:, cut], wide_cosine, wide_sine)
        pair = jnp.where(lane_of // ROTARY == head % 2, pair, 0.0).astype(BF16)
        query[head, :, :CONTENT] = content[:, head * CONTENT : (head + 1) * CONTENT]
        query[head, :, CONTENT:] = pair
    highest[...] = jnp.full(highest.shape, MASKED, F32)
    denominator[...] = jnp.zeros(denominator.shape, F32)
    summed[...] = jnp.zeros(summed.shape, F32)
    loads[3].wait()
    value_turned[...] = value_ref[...].astype(F32).T.astype(BF16)
    loads[4].wait()
    anchor = me * length

    def absorb(slot, block_ref):
        shared = block_ref[:, :rank]
        turn = block_ref[:, rank:]
        keys = jnp.dot(shared, key_ref[...], preferred_element_type=F32).astype(BF16)
        values = lax.dot_general(
            value_turned[...], shared, (((1,), (1,)), ((), ())), preferred_element_type=F32
        ).astype(BF16)
        shape = (length, length)
        key_places = anchor - slot * length + lax.broadcasted_iota(jnp.int32, shape, 0)
        visible = key_places >= start_ref[...]
        if isinstance(slot, int) and slot == 0:
            visible = visible & (
                lax.broadcasted_iota(jnp.int32, shape, 0)
                <= lax.broadcasted_iota(jnp.int32, shape, 1)
            )
        for head in range(heads):
            cut = slice(head * CONTENT, (head + 1) * CONTENT)
            joined = jnp.concatenate([keys[:, cut], turn], axis=1)
            scores = lax.dot_general(
                joined, query[head], (((1,), (1,)), ((), ())), preferred_element_type=F32
            )
            scores = jnp.where(visible, scores * scale, MASKED)
            before = highest[head]
            after = jnp.maximum(before, jnp.max(scores, axis=0, keepdims=True))
            factor = jnp.exp2(before - after)
            weights = jnp.exp2(scores - after)
            highest[head] = after
            denominator[head] = denominator[head] * factor + jnp.sum(
                weights, axis=0, keepdims=True
            )
            summed[head] = summed[head] * factor + jnp.dot(
                values[cut, :], weights.astype(BF16), preferred_element_type=F32
            )

    def absorb_slot(slot):
        absorb(slot, win_ref.at[slot])

    absorb(0, pay_ref)

    @on_core(1)
    def _():
        d_copy(0, 1).wait_recv()
        absorb_slot(1)

    def absorb_sibling(lane):
        from_sibling(lane)
        absorb_slot(2 * lane - 1 + 2 * core)

    @pl.when(has(1))
    def _():
        arrived(1)
        relay(1)

    @pl.when(has(2))
    def _():
        arrived(2)

    @pl.when(has(1))
    def _():
        finish(1)
        absorb_slot(2)

    @pl.when(has(2))
    def _():
        relay(2)

    @pl.when(has(1))
    def _():
        absorb_sibling(1)

    @pl.when(has(2))
    def _():
        finish(2)

    @pl.when(has(3))
    def _():
        arrived(3)

    @on_core(0, has(4))
    def _():
        arrived(4)

    @pl.when(has(2))
    def _():
        absorb_slot(4)

    @pl.when(has(3))
    def _():
        relay(3)

    @on_core(0, has(4))
    def _():
        relay(4)

    @pl.when(has(2))
    def _():
        absorb_sibling(2)

    @pl.when(has(3))
    def _():
        finish(3)
        absorb_slot(6)
        absorb_sibling(3)

    @on_core(0, has(4))
    def _():
        finish(4)
        absorb_slot(7)

    for head in range(heads):
        cut = slice(head * CONTENT, (head + 1) * CONTENT)
        attended[:, cut] = (summed[head] / denominator[head]).T.astype(BF16)
    loads[5].wait()

    size = length // CHUNKS
    half, piece = model // 4, model // 8
    bit = col // 2
    gray = lax.rem(col + bit, 2)
    near = (col + 1 - 2 * lax.rem(col, 2), ring - 1 - col)
    keep = (gray, bit)
    sub = (bit, gray)

    def part(chunk):
        return pl.ds(chunk * size, size)

    def half_at(side, which):
        return pl.multiple_of(side * (model // 2) + which * half, half)

    def piece_at(side, which, sub_which):
        return pl.multiple_of(side * (model // 2) + which * half + sub_which * piece, piece)

    def copy(kind, side, chunk, src, dst, partner):
        return copy_to(
            src, dst, send.at[kind, side, chunk], recv.at[kind, side, chunk], me, partner
        )

    def stage_one(side, chunk):
        return copy(
            0, side, chunk, term.at[side, part(chunk)], first.at[side, part(chunk)], near[side]
        )

    def stage_two(side, chunk):
        return copy(
            1, side, chunk, held.at[side, part(chunk)], second.at[side, part(chunk)], near[1 - side]
        )

    def gather(kind, side, chunk):
        which = 1 - sub[side] if kind == 4 else sub[side]
        ref = out_ref.at[part(chunk), pl.ds(piece_at(side, keep[side], which), piece)]
        return copy(kind, side, chunk, ref, ref, near[1 - side] if kind == 2 else near[side])

    def project(chunk, at, width):
        return jnp.dot(
            attended[part(chunk), :], weight_ref[:, pl.ds(at, width)], preferred_element_type=F32
        ).astype(BF16)

    for chunk in range(CHUNKS):
        for side in (0, 1):
            term[side, part(chunk), :] = project(chunk, half_at(side, 1 - keep[side]), half)
            stage_one(side, chunk).start()

    for chunk in range(CHUNKS):
        for side in (0, 1):
            theirs = pl.multiple_of((1 - sub[side]) * piece, piece)
            mine = project(chunk, piece_at(side, keep[side], 1 - sub[side]), piece)
            stage_one(side, chunk).wait_recv()
            held[side, part(chunk), :] = (
                mine.astype(F32) + first[side, part(chunk), pl.ds(theirs, piece)].astype(F32)
            ).astype(BF16)
            stage_two(side, chunk).start()

    for chunk in range(CHUNKS):
        for side in (0, 1):
            ours = pl.multiple_of(sub[side] * piece, piece)
            at = piece_at(side, keep[side], sub[side])
            mine = project(chunk, at, piece).astype(F32)
            mine = mine + first[side, part(chunk), pl.ds(ours, piece)].astype(F32)
            stage_two(side, chunk).wait_recv()
            out_ref[part(chunk), pl.ds(at, piece)] = (
                mine + second[side, part(chunk), :].astype(F32)
            ).astype(BF16)
            gather(2, side, chunk).start()
            gather(3, side, chunk).start()

    for chunk in range(CHUNKS):
        for side in (0, 1):
            gather(2, side, chunk).wait_recv()
            gather(4, side, chunk).start()

    for chunk in range(CHUNKS):
        for side in (0, 1):
            gather(3, side, chunk).wait_recv()
            gather(4, side, chunk).wait_recv()
            stage_one(side, chunk).wait_send()
            stage_two(side, chunk).wait_send()
            for kind in (2, 3, 4):
                gather(kind, side, chunk).wait_send()

    for steps in (1, 2, 3):

        @pl.when(feeds(steps))
        def _():
            y_copy(steps).wait_send()

        @pl.when(has(steps))
        def _():
            for kind in range(4):
                x_copy(steps, kind).wait_send()
            d_copy(steps, -1).wait_send()

    @pl.when(far)
    def _():
        y_copy(4).wait_send()

    @on_core(0)
    def _():
        d_copy(0, 1).wait_send()

    @on_core(0, has(4))
    def _():
        for kind in range(4):
            x_copy(4, kind).wait_send()


def on_device(
    query_latent,
    shared_latent,
    rotary_key,
    document_start,
    query_gain,
    shared_gain,
    content_weight,
    rotary_weight,
    key_weight,
    value_weight,
    output_weight,
):
    length, query_rank = query_latent.shape
    rank = shared_latent.shape[1]
    model = output_weight.shape[1]
    heads = key_weight.shape[1] // CONTENT
    width = rank + 2 * ROTARY
    places = lax.axis_index("sp") * length + jnp.arange(length, dtype=jnp.int32)
    frequency = 1.0 / THETA ** (jnp.arange(0, ROTARY, 2, dtype=F32) / ROTARY)
    angles = frequency[:, None] * places.astype(F32)[None, :]
    vmem, dma = pltpu.VMEM, pltpu.SemaphoreType.DMA
    return pl.pallas_call(
        mixed_kernel,
        out_shape=jax.ShapeDtypeStruct((length, model), BF16),
        in_specs=[FAR] + [WHOLE] * 7 + [FAR] * 5,
        out_specs=WHOLE,
        scratch_shapes=[
            vmem((length, query_rank), BF16),
            vmem(content_weight.shape, BF16),
            vmem(rotary_weight.shape, BF16),
            vmem(key_weight.shape, BF16),
            vmem(value_weight.shape, BF16),
            vmem(output_weight.shape, BF16),
            vmem(value_weight.shape[::-1], BF16),
            vmem((length, width), BF16),
            vmem((SPAN, length, width), BF16),
            vmem((heads, length, 2 * CONTENT), BF16),
            vmem((heads, 1, length), F32),
            vmem((heads, 1, length), F32),
            vmem((heads, CONTENT, length), F32),
            vmem((length, heads * CONTENT), BF16),
            vmem((2, length, model // 4), BF16),
            vmem((2, length, model // 4), BF16),
            vmem((2, length, model // 8), BF16),
            vmem((2, length, model // 8), BF16),
            dma((6,)),
            dma((5,)),
            dma((5,)),
            dma((5, 4)),
            dma((5, 4)),
            dma((4,)),
            dma((4,)),
            dma((5, 2, CHUNKS)),
            dma((5, 2, CHUNKS)),
        ],
        compiler_params=pltpu.CompilerParams(
            collective_id=0, has_side_effects=True, vmem_limit_bytes=46 * 2**20
        ),
        name="mixed",
    )(
        query_latent,
        shared_latent,
        rotary_key.T,
        document_start[None, :],
        jnp.cos(angles),
        jnp.sin(angles),
        query_gain[None, :],
        shared_gain[None, :],
        content_weight,
        rotary_weight,
        key_weight,
        value_weight,
        output_weight,
    )


def solution(mesh):
    return jax.shard_map(
        on_device,
        mesh=mesh,
        in_specs=(
            P("sp", None),
            P("sp", None),
            P("sp", None),
            P("sp"),
            P(),
            P(),
            P(None, "tp"),
            P(None, "tp"),
            P(None, "tp"),
            P(None, "tp"),
            P("tp", None),
        ),
        out_specs=P("sp", None),
        check_vma=False,
    )
```

time: 217 us -> 93.3 us (0.43)
  the two profiles are of different devices: /device:TPU:1 before, /device:TPU:560 now
where the time goes in v2:
time: 93.3 us; the launch traced here: 92.7 us
  Pallas kernels  82 us (88%)
  local copies, waits for them, and re-layouts  10.5 us (11%)
    pallas_call x1, Pallas kernels, on_device(): pl.pallas_call(mixed_kernel, out_shape=jax.ShapeDtypeStruct((length, mode...  82 us
    unnamed x21, local copies, waits for them, and re-layouts  10.5 us

profile of v2, /device:TPU:560, one launch (start us, length us, event | category | flops | bytes accessed | tf_op | source)
XLA Modules:
  0.0 92.7 jit_solution(5599708560540792780)
XLA Ops:
  0.0 0.2 multiply_sine_fusion
  0.2 0.0 copy-start
  0.2 1.2 %copy-done = bf16[1024,512]{1,0:T(8,128)(2,1)S(1)} copy-done((bf16[1024,512]{1,0:T(8,128)(2,1)S(1)}, bf16[1024,512]{1,0:T(8,128)(2,1)}, u32[]{:S(2)}) %copy-start) | copy-done | bytes 1048600
  1.5 0.0 copy-start.1
  1.5 1.0 %copy-done.1 = bf16[256,1024]{1,0:T(8,128)(2,1)S(1)} copy-done((bf16[256,1024]{1,0:T(8,128)(2,1)S(1)}, bf16[256,1024]{1,0:T(8,128)(2,1)}, u32[]{:S(2)}) %copy-start.1) | copy-done | bytes 524312
  2.5 0.0 copy-start.2
  2.5 1.0 %copy-done.2 = bf16[1024,256]{1,0:T(8,128)(2,1)S(1)} copy-done((bf16[1024,256]{1,0:T(8,128)(2,1)S(1)}, bf16[1024,256]{1,0:T(8,128)(2,1)}, u32[]{:S(2)}) %copy-start.2) | copy-done | bytes 524312
  3.5 0.0 copy-start.3
  3.5 1.0 %copy-done.3 = bf16[512,512]{1,0:T(8,128)(2,1)S(1)} copy-done((bf16[512,512]{1,0:T(8,128)(2,1)S(1)}, bf16[512,512]{1,0:T(8,128)(2,1)}, u32[]{:S(2)}) %copy-start.3) | copy-done | bytes 524312
  4.6 0.0 copy-start.4
  4.6 1.0 %copy-done.4 = bf16[512,512]{1,0:T(8,128)(2,1)S(1)} copy-done((bf16[512,512]{1,0:T(8,128)(2,1)S(1)}, bf16[512,512]{1,0:T(8,128)(2,1)}, u32[]{:S(2)}) %copy-start.4) | copy-done | bytes 524312
  5.6 0.0 copy-start.5
  5.6 0.9 %copy-done.5 = bf16[256,512]{1,0:T(8,128)(2,1)S(1)} copy-done((bf16[256,512]{1,0:T(8,128)(2,1)S(1)}, bf16[256,512]{1,0:T(8,128)(2,1)}, u32[]{:S(2)}) %copy-start.5) | copy-done | bytes 262168
  6.6 0.0 copy-start.6
  6.6 0.8 copy-done.6
  7.3 0.0 copy-start.7
  7.3 0.7 copy-done.7
  8.0 0.0 copy-start.8
  8.0 0.7 copy-done.8
  8.7 0.0 copy-start.9
  8.7 0.7 copy-done.9
  9.4 82.0 %mixed.1 = bf16[256,4096]{1,0:T(8,128)(2,1)S(1)} custom-call(bf16[256,1024]{1,0:T(8,128)(2,1)S(1)} %copy-done.1, bf16[256,512]{1,0:T(8,128)(2,1)S(1)} %copy-done.5, bf16[64,256]{1,0:T(8,128)(2,1)S(1)} %bitcast.4, s32[1,256]{1,0:T(1,128)S(1)} %bitcast.7, f32[32,256]{1,0:T(8,128)S(1)} %get-tuple-element.6.cos_ref, f32[32,256]{1,0:T(8,128)S(1)} %get-tuple-element.5.sin_ref, ...), custom_call_target="tpu_custom_call" | custom-call | tf_op jit(solution)/shard_map/mixed/pallas_call | solution.py:500
  91.4 1.3 %copy.13 = bf16[256,4096]{1,0:T(8,128)(2,1)} copy(bf16[256,4096]{1,0:T(8,128)(2,1)S(1)} %mixed.1) | data formatting | bytes 4194304
  (2 shorter events, 0.0 us)
Async XLA Ops:
  0.2 1.2 %copy-start = (bf16[1024,512]{1,0:T(8,128)(2,1)S(1)}, bf16[1024,512]{1,0:T(8,128)(2,1)}, u32[]{:S(2)}) copy-start(bf16[1024,512]{1,0:T(8,128)(2,1)} %content_hbm.1) | copy-start | bytes 3145732
  1.5 1.0 %copy-start.1 = (bf16[256,1024]{1,0:T(8,128)(2,1)S(1)}, bf16[256,1024]{1,0:T(8,128)(2,1)}, u32[]{:S(2)}) copy-start(bf16[256,1024]{1,0:T(8,128)(2,1)} %latent_hbm.1) | copy-start | bytes 1572868
  2.5 1.0 %copy-start.2 = (bf16[1024,256]{1,0:T(8,128)(2,1)S(1)}, bf16[1024,256]{1,0:T(8,128)(2,1)}, u32[]{:S(2)}) copy-start(bf16[1024,256]{1,0:T(8,128)(2,1)} %rotary_weight_hbm.1) | copy-start | bytes 1572868
  3.5 1.0 %copy-start.3 = (bf16[512,512]{1,0:T(8,128)(2,1)S(1)}, bf16[512,512]{1,0:T(8,128)(2,1)}, u32[]{:S(2)}) copy-start(bf16[512,512]{1,0:T(8,128)(2,1)} %key_hbm.1) | copy-start | bytes 1572868
  4.6 1.0 %copy-start.4 = (bf16[512,512]{1,0:T(8,128)(2,1)S(1)}, bf16[512,512]{1,0:T(8,128)(2,1)}, u32[]{:S(2)}) copy-start(bf16[512,512]{1,0:T(8,128)(2,1)} %value_hbm.1) | copy-start | bytes 1572868
  5.6 0.9 %copy-start.5 = (bf16[256,512]{1,0:T(8,128)(2,1)S(1)}, bf16[256,512]{1,0:T(8,128)(2,1)}, u32[]{:S(2)}) copy-start(bf16[256,512]{1,0:T(8,128)(2,1)} %shared_ref.1) | copy-start | bytes 786436
  6.6 0.8 copy-start.6
  7.3 0.7 copy-start.7
  8.0 0.7 copy-start.8
  8.7 0.7 copy-start.9

commit v3 on v2

--- a/solution.py
+++ b/solution.py
@@ -128,7 +128,7 @@
     greet(me, east)
     greet(me, west)
     greet(sibling, col)
-    for steps in (1, 2, 3):
+    for steps in (1, 2):
 
         @pl.when(has(steps))
         def _():
@@ -136,7 +136,7 @@
 
     @pl.when((core == 0) & has(4))
     def _():
-        greet(me - 7, col)
+        greet(me - 3, col)
 
     pay_ref[:, :rank] = rms_scale(shared_ref[...], shared_gain_ref[...])
     leading = rotary_ref[: ROTARY // 2, :].astype(F32)
@@ -150,9 +150,10 @@
 
     def y_copy(steps):
         part = rows(col, 0, quarter)
-        slot, to = (2 * steps, me + 2 * steps) if steps < 4 else (7, me + 7)
+        src = pay_ref.at[part] if steps < 3 else win_ref.at[4, part]
+        slot, to = ((2, me + 2), (4, me + 4), (6, me + 2), (7, me + 3))[steps - 1]
         return copy_to(
-            pay_ref.at[part], win_ref.at[slot, part], y_send.at[steps], y_recv.at[steps], to, col
+            src, win_ref.at[slot, part], y_send.at[steps], y_recv.at[steps], to, col
         )
 
     def x_copy(lane, kind):
@@ -178,18 +179,14 @@
         mine = core == which
         return pl.when(mine if also is None else mine & also)
 
-    far = (core == 1) & feeds(4)
-    number = 3 + jnp.minimum(3, chips - 1 - chip) + far.astype(jnp.int32)
+    far = (core == 1) & has(2) & feeds(2)
+    number = 3 + jnp.minimum(2, chips - 1 - chip) + far.astype(jnp.int32)
     pl.semaphore_wait(barrier, number)
-    for steps in (1, 2, 3):
+    for steps in (1, 2):
 
         @pl.when(feeds(steps))
         def _():
             y_copy(steps).start()
-
-    @pl.when(far)
-    def _():
-        y_copy(4).start()
 
     @on_core(0)
     def _():
@@ -197,6 +194,16 @@
 
     def arrived(lane):
         y_copy(lane).wait_recv()
+        if lane == 2:
+
+            @pl.when(feeds(1))
+            def _():
+                y_copy(3).start()
+
+            @pl.when(far)
+            def _():
+                y_copy(4).start()
+
         x_copy(lane, 0).start()
         x_copy(lane, 1).start()
 
@@ -299,66 +306,31 @@
         from_sibling(lane)
         absorb_slot(2 * lane - 1 + 2 * core)
 
-    @pl.when(has(1))
-    def _():
-        arrived(1)
-        relay(1)
-
-    @pl.when(has(2))
-    def _():
-        arrived(2)
-
-    @pl.when(has(1))
-    def _():
-        finish(1)
-        absorb_slot(2)
-
-    @pl.when(has(2))
-    def _():
-        relay(2)
-
-    @pl.when(has(1))
-    def _():
-        absorb_sibling(1)
-
-    @pl.when(has(2))
-    def _():
-        finish(2)
-
-    @pl.when(has(3))
-    def _():
-        arrived(3)
-
-    @on_core(0, has(4))
-    def _():
-        arrived(4)
-
-    @pl.when(has(2))
-    def _():
-        absorb_slot(4)
-
-    @pl.when(has(3))
-    def _():
-        relay(3)
-
-    @on_core(0, has(4))
-    def _():
-        relay(4)
-
-    @pl.when(has(2))
-    def _():
-        absorb_sibling(2)
-
-    @pl.when(has(3))
-    def _():
-        finish(3)
-        absorb_slot(6)
-        absorb_sibling(3)
-
-    @on_core(0, has(4))
-    def _():
-        finish(4)
-        absorb_slot(7)
+    def steps_of(lane, *steps):
+        @pl.when((core == 0) & has(4) if lane == 4 else has(lane))
+        def _():
+            for step in steps:
+                step(lane)
+
+    def absorb_lane(lane):
+        absorb_slot(2 * lane if lane < 4 else 7)
+
+    steps_of(1, arrived)
+    steps_of(2, arrived)
+    steps_of(1, relay)
+    steps_of(2, relay)
+    steps_of(1, finish, absorb_lane)
+    steps_of(3, arrived)
+    steps_of(4, arrived)
+    steps_of(2, finish)
+    steps_of(1, absorb_sibling)
+    steps_of(2, absorb_lane)
+    steps_of(3, relay)
+    steps_of(4, relay)
+    steps_of(2, absorb_sibling)
+    steps_of(3, finish, absorb_lane)
+    steps_of(4, finish, absorb_lane)
+    steps_of(3, absorb_sibling)
 
     for head in range(heads):
         cut = slice(head * CONTENT, (head + 1) * CONTENT)
@@ -451,7 +423,7 @@
 
     for steps in (1, 2, 3):
 
-        @pl.when(feeds(steps))
+        @pl.when(feeds(steps) if steps < 3 else has(2) & feeds(1))
         def _():
             y_copy(steps).wait_send()
 
@@ -497,6 +469,24 @@
     frequency = 1.0 / THETA ** (jnp.arange(0, ROTARY, 2, dtype=F32) / ROTARY)
     angles = frequency[:, None] * places.astype(F32)[None, :]
     vmem, dma = pltpu.VMEM, pltpu.SemaphoreType.DMA
+    pinned = [
+        pltpu.with_memory_space_constraint(item, pltpu.HBM)
+        for item in (
+            query_latent,
+            shared_latent,
+            rotary_key.T,
+            document_start[None, :],
+            jnp.cos(angles),
+            jnp.sin(angles),
+            query_gain[None, :],
+            shared_gain[None, :],
+            content_weight,
+            rotary_weight,
+            key_weight,
+            value_weight,
+            output_weight,
+        )
+    ]
     return pl.pallas_call(
         mixed_kernel,
         out_shape=jax.ShapeDtypeStruct((length, model), BF16),
@@ -536,19 +526,8 @@
         ),
         name="mixed",
     )(
-        query_latent,
-        shared_latent,
-        rotary_key.T,
-        document_start[None, :],
-        jnp.cos(angles),
-        jnp.sin(angles),
-        query_gain[None, :],
-        shared_gain[None, :],
-        content_weight,
-        rotary_weight,
-        key_weight,
-        value_weight,
-        output_weight,
+
+        *pinned,
     )
 
 

time: 93.3 us -> 75.8 us (0.81)
  the two profiles are of different devices: /device:TPU:560 before, /device:TPU:256 now
where the time goes in v3:
time: 75.8 us; the launch traced here: 75.6 us
  Pallas kernels  73.4 us (97%)
  local copies, waits for them, and re-layouts  1.32 us (2%)
  other arithmetic  0.85 us (1%)
    pallas_call x1, Pallas kernels, on_device(): pl.pallas_call(mixed_kernel, out_shape=jax.ShapeDtypeStruct((length, mode...  73.4 us

profile of v3, /device:TPU:256, one launch (start us, length us, event | category | flops | bytes accessed | tf_op | source)
XLA Modules:
  0.0 75.6 jit_solution(189797050534774609)
XLA Ops:
  0.0 0.8 %multiply_sine_fusion = (f32[32,256]{1,0:T(8,128)}, f32[32,256]{1,0:T(8,128)}) fusion(f32[256]{0:T(256)S(1)} %add_convert_fusion, f32[32]{0:T(128)S(1)} %negate_power_fusion), kind=kLoop, calls=%fused_computation | loop fusion | flops 8192 | bytes 66688 | tf_op jit(solution)/shard_map/sin | solution.py:480
  0.9 73.4 %mixed.1 = bf16[256,4096]{1,0:T(8,128)(2,1)S(1)} custom-call(bf16[256,1024]{1,0:T(8,128)(2,1)} %latent_hbm.1, bf16[256,512]{1,0:T(8,128)(2,1)} %shared_ref.1, bf16[64,256]{1,0:T(8,128)(2,1)} %bitcast.4, s32[1,256]{1,0:T(1,128)} %bitcast.7, f32[32,256]{1,0:T(8,128)} %get-tuple-element.6.cos_ref, f32[32,256]{1,0:T(8,128)} %get-tuple-element.5.sin_ref, ...), custom_call_target="tpu_custom_call" | custom-call | tf_op jit(solution)/shard_map/mixed/pallas_call | solution.py:490
  74.3 1.3 %copy.13 = bf16[256,4096]{1,0:T(8,128)(2,1)} copy(bf16[256,4096]{1,0:T(8,128)(2,1)S(1)} %mixed.1) | data formatting | bytes 4194304
  (2 shorter events, 0.0 us)

commit v4 on v3

--- a/solution.py
+++ b/solution.py
@@ -48,6 +48,19 @@
 
 def mixed_kernel(
     latent_hbm,
+    shared_hbm,
+    rotary_hbm,
+    start_hbm,
+    cos_hbm,
+    sin_hbm,
+    query_gain_hbm,
+    shared_gain_hbm,
+    content_hbm,
+    rotary_weight_hbm,
+    key_hbm,
+    value_hbm,
+    output_hbm,
+    out_ref,
     shared_ref,
     rotary_ref,
     start_ref,
@@ -55,12 +68,6 @@
     sin_ref,
     query_gain_ref,
     shared_gain_ref,
-    content_hbm,
-    rotary_weight_hbm,
-    key_hbm,
-    value_hbm,
-    output_hbm,
-    out_ref,
     latent_ref,
     content_ref,
     rotary_weight_ref,
@@ -75,8 +82,8 @@
     denominator,
     summed,
     attended,
-    term,
-    first,
+    near_attended,
+    near_weight,
     second,
     held,
     load_sem,
@@ -86,6 +93,10 @@
     x_recv,
     d_send,
     d_recv,
+    w_send,
+    w_recv,
+    s_send,
+    s_recv,
     send,
     recv,
 ):
@@ -99,6 +110,16 @@
     heads = key_ref.shape[1] // CONTENT
     model = out_ref.shape[1]
     quarter, eighth = length // 4, length // 8
+    size = length // CHUNKS
+    half, piece = model // 4, model // 8
+    bit = col // 2
+    gray = lax.rem(col + bit, 2)
+    near = (col + 1 - 2 * lax.rem(col, 2), ring - 1 - col)
+    keep = (gray, bit)
+    sub = (bit, gray)
+
+    def piece_at(side, which, sub_which):
+        return pl.multiple_of(side * (model // 2) + which * half + sub_which * piece, piece)
 
     def load(index, src, dst):
         return pltpu.make_async_copy(src, dst, load_sem.at[index])
@@ -111,7 +132,16 @@
         load(4, key_hbm, key_ref),
         load(5, output_hbm, weight_ref),
     ]
-    for item in loads:
+    small = [
+        load(6, shared_hbm, shared_ref),
+        load(7, rotary_hbm, rotary_ref),
+        load(8, cos_hbm, cos_ref),
+        load(9, sin_hbm, sin_ref),
+        load(10, shared_gain_hbm, shared_gain_ref),
+        load(11, query_gain_hbm, query_gain_ref),
+        load(12, start_hbm, start_ref),
+    ]
+    for item in small + loads:
         item.start()
 
     barrier = pltpu.get_barrier_semaphore()
@@ -138,6 +168,8 @@
     def _():
         greet(me - 3, col)
 
+    for item in small:
+        item.wait()
     pay_ref[:, :rank] = rms_scale(shared_ref[...], shared_gain_ref[...])
     leading = rotary_ref[: ROTARY // 2, :].astype(F32)
     trailing = rotary_ref[ROTARY // 2 :, :].astype(F32)
@@ -158,14 +190,15 @@
 
     def x_copy(lane, kind):
         slot = 2 * lane if lane < 4 else 7
-        if kind == 0:
-            part, to = rows(col, 0, quarter), east
-        elif kind == 1:
-            part, to = rows(col, 0, quarter), west
-        elif kind == 2:
-            part, to = rows(west, 0, eighth), east
-        else:
-            part, to = rows(east, eighth, eighth), west
+        owner, offset, to = (
+            (col, 0, east),
+            (col, eighth, west),
+            (west, 0, east),
+            (east, eighth, west),
+            (col, eighth, east),
+            (col, 0, west),
+        )[kind]
+        part = rows(owner, offset, eighth)
         ref = win_ref.at[slot, part]
         return copy_to(ref, ref, x_send.at[lane, kind], x_recv.at[lane, kind], me, to)
 
@@ -182,7 +215,7 @@
     far = (core == 1) & has(2) & feeds(2)
     number = 3 + jnp.minimum(2, chips - 1 - chip) + far.astype(jnp.int32)
     pl.semaphore_wait(barrier, number)
-    for steps in (1, 2):
+    for steps in (2, 1):
 
         @pl.when(feeds(steps))
         def _():
@@ -192,6 +225,32 @@
     def _():
         d_copy(0, 1).start()
 
+    depth = weight_ref.shape[0] // 2
+    core_rows = pl.ds(pl.multiple_of(core * depth, depth), depth)
+
+    def w_copy(turn, side):
+        at = piece_at(side, 1 - keep[side], 1 - sub[side] if turn == 0 else sub[side])
+        return copy_to(
+            output_hbm.at[core_rows, pl.ds(at, piece)],
+            near_weight.at[turn, side, core_rows],
+            w_send.at[turn, side],
+            w_recv.at[turn, side],
+            me,
+            near[side],
+        )
+
+    def s_copy(turn, side):
+        ref = near_weight.at[turn, side, core_rows]
+        return copy_to(ref, ref, s_send.at[turn, side], s_recv.at[turn, side], sibling, col)
+
+    def share(turn):
+        for side in (0, 1):
+            w_copy(turn, side).wait_recv()
+            s_copy(turn, side).start()
+
+    for side in (0, 1):
+        w_copy(0, side).start()
+
     def arrived(lane):
         y_copy(lane).wait_recv()
         if lane == 2:
@@ -204,8 +263,8 @@
             def _():
                 y_copy(4).start()
 
-        x_copy(lane, 0).start()
-        x_copy(lane, 1).start()
+        for kind in (0, 1, 4, 5):
+            x_copy(lane, kind).start()
 
     def relay(lane):
         x_copy(lane, 0).wait_recv()
@@ -214,8 +273,8 @@
         x_copy(lane, 3).start()
 
     def finish(lane):
-        x_copy(lane, 2).wait_recv()
-        x_copy(lane, 3).wait_recv()
+        for kind in (4, 5, 2, 3):
+            x_copy(lane, kind).wait_recv()
         if lane < 4:
 
             @on_core(0)
@@ -315,44 +374,33 @@
     def absorb_lane(lane):
         absorb_slot(2 * lane if lane < 4 else 7)
 
+    steps_of(2, arrived)
     steps_of(1, arrived)
-    steps_of(2, arrived)
+    steps_of(2, relay)
     steps_of(1, relay)
-    steps_of(2, relay)
-    steps_of(1, finish, absorb_lane)
     steps_of(3, arrived)
     steps_of(4, arrived)
-    steps_of(2, finish)
-    steps_of(1, absorb_sibling)
-    steps_of(2, absorb_lane)
+    steps_of(2, finish, absorb_lane)
+    steps_of(1, finish)
     steps_of(3, relay)
     steps_of(4, relay)
+    for side in (0, 1):
+        w_copy(1, side).start()
+    steps_of(1, absorb_lane)
+    share(0)
     steps_of(2, absorb_sibling)
-    steps_of(3, finish, absorb_lane)
+    steps_of(3, finish)
+    steps_of(1, absorb_sibling)
+    steps_of(3, absorb_lane)
     steps_of(4, finish, absorb_lane)
     steps_of(3, absorb_sibling)
 
     for head in range(heads):
         cut = slice(head * CONTENT, (head + 1) * CONTENT)
         attended[:, cut] = (summed[head] / denominator[head]).T.astype(BF16)
-    loads[5].wait()
-
-    size = length // CHUNKS
-    half, piece = model // 4, model // 8
-    bit = col // 2
-    gray = lax.rem(col + bit, 2)
-    near = (col + 1 - 2 * lax.rem(col, 2), ring - 1 - col)
-    keep = (gray, bit)
-    sub = (bit, gray)
 
     def part(chunk):
         return pl.ds(chunk * size, size)
-
-    def half_at(side, which):
-        return pl.multiple_of(side * (model // 2) + which * half, half)
-
-    def piece_at(side, which, sub_which):
-        return pl.multiple_of(side * (model // 2) + which * half + sub_which * piece, piece)
 
     def copy(kind, side, chunk, src, dst, partner):
         return copy_to(
@@ -361,7 +409,12 @@
 
     def stage_one(side, chunk):
         return copy(
-            0, side, chunk, term.at[side, part(chunk)], first.at[side, part(chunk)], near[side]
+            0,
+            side,
+            chunk,
+            attended.at[part(chunk)],
+            near_attended.at[side, part(chunk)],
+            near[side],
         )
 
     def stage_two(side, chunk):
@@ -374,32 +427,50 @@
         ref = out_ref.at[part(chunk), pl.ds(piece_at(side, keep[side], which), piece)]
         return copy(kind, side, chunk, ref, ref, near[1 - side] if kind == 2 else near[side])
 
-    def project(chunk, at, width):
-        return jnp.dot(
-            attended[part(chunk), :], weight_ref[:, pl.ds(at, width)], preferred_element_type=F32
-        ).astype(BF16)
+    def project(chunk, at):
+        return (
+            jnp.dot(
+                attended[part(chunk), :],
+                weight_ref[:, pl.ds(at, piece)],
+                preferred_element_type=F32,
+            )
+            .astype(BF16)
+            .astype(F32)
+        )
+
+    def project_near(turn, side, chunk):
+        return (
+            jnp.dot(
+                near_attended[side, part(chunk), :],
+                near_weight[turn, side],
+                preferred_element_type=F32,
+            )
+            .astype(BF16)
+            .astype(F32)
+        )
 
     for chunk in range(CHUNKS):
         for side in (0, 1):
-            term[side, part(chunk), :] = project(chunk, half_at(side, 1 - keep[side]), half)
             stage_one(side, chunk).start()
+    share(1)
+    loads[5].wait()
+    for side in (0, 1):
+        s_copy(0, side).wait_recv()
 
     for chunk in range(CHUNKS):
         for side in (0, 1):
-            theirs = pl.multiple_of((1 - sub[side]) * piece, piece)
-            mine = project(chunk, piece_at(side, keep[side], 1 - sub[side]), piece)
+            mine = project(chunk, piece_at(side, keep[side], 1 - sub[side]))
             stage_one(side, chunk).wait_recv()
-            held[side, part(chunk), :] = (
-                mine.astype(F32) + first[side, part(chunk), pl.ds(theirs, piece)].astype(F32)
-            ).astype(BF16)
+            held[side, part(chunk), :] = (mine + project_near(0, side, chunk)).astype(BF16)
             stage_two(side, chunk).start()
+
+    for side in (0, 1):
+        s_copy(1, side).wait_recv()
 
     for chunk in range(CHUNKS):
         for side in (0, 1):
-            ours = pl.multiple_of(sub[side] * piece, piece)
             at = piece_at(side, keep[side], sub[side])
-            mine = project(chunk, at, piece).astype(F32)
-            mine = mine + first[side, part(chunk), pl.ds(ours, piece)].astype(F32)
+            mine = project(chunk, at) + project_near(1, side, chunk)
             stage_two(side, chunk).wait_recv()
             out_ref[part(chunk), pl.ds(at, piece)] = (
                 mine + second[side, part(chunk), :].astype(F32)
@@ -421,6 +492,10 @@
             for kind in (2, 3, 4):
                 gather(kind, side, chunk).wait_send()
 
+    for turn in (0, 1):
+        for side in (0, 1):
+            w_copy(turn, side).wait_send()
+            s_copy(turn, side).wait_send()
     for steps in (1, 2, 3):
 
         @pl.when(feeds(steps) if steps < 3 else has(2) & feeds(1))
@@ -429,7 +504,7 @@
 
         @pl.when(has(steps))
         def _():
-            for kind in range(4):
+            for kind in range(6):
                 x_copy(steps, kind).wait_send()
             d_copy(steps, -1).wait_send()
 
@@ -443,7 +518,7 @@
 
     @on_core(0, has(4))
     def _():
-        for kind in range(4):
+        for kind in range(6):
             x_copy(4, kind).wait_send()
 
 
@@ -490,9 +565,16 @@
     return pl.pallas_call(
         mixed_kernel,
         out_shape=jax.ShapeDtypeStruct((length, model), BF16),
-        in_specs=[FAR] + [WHOLE] * 7 + [FAR] * 5,
+        in_specs=[FAR] * 13,
         out_specs=WHOLE,
         scratch_shapes=[
+            vmem((length, rank), BF16),
+            vmem((ROTARY, length), BF16),
+            vmem((1, length), jnp.int32),
+            vmem((ROTARY // 2, length), F32),
+            vmem((ROTARY // 2, length), F32),
+            vmem((1, query_rank), F32),
+            vmem((1, rank), F32),
             vmem((length, query_rank), BF16),
             vmem(content_weight.shape, BF16),
             vmem(rotary_weight.shape, BF16),
@@ -507,17 +589,21 @@
             vmem((heads, 1, length), F32),
             vmem((heads, CONTENT, length), F32),
             vmem((length, heads * CONTENT), BF16),
-            vmem((2, length, model // 4), BF16),
-            vmem((2, length, model // 4), BF16),
+            vmem((2, length, heads * CONTENT), BF16),
+            vmem((2, 2, output_weight.shape[0], model // 8), BF16),
             vmem((2, length, model // 8), BF16),
             vmem((2, length, model // 8), BF16),
-            dma((6,)),
+            dma((13,)),
             dma((5,)),
             dma((5,)),
-            dma((5, 4)),
-            dma((5, 4)),
+            dma((5, 6)),
+            dma((5, 6)),
             dma((4,)),
             dma((4,)),
+            dma((2, 2)),
+            dma((2, 2)),
+            dma((2, 2)),
+            dma((2, 2)),
             dma((5, 2, CHUNKS)),
             dma((5, 2, CHUNKS)),
         ],

time: 75.8 us -> 66.7 us (0.88)
  Pallas kernels: 73.4 us -> 64.4 us
    pallas_call x1, Pallas kernels: 73.4 us -> 64.4 us  [on_device(): pl.pallas_call(mixed_kernel, out_shape=jax.ShapeDtypeStruct((length, mode...]
where the time goes in v4:
time: 66.7 us; the launch traced here: 66.6 us
  Pallas kernels  64.4 us (97%)
  local copies, waits for them, and re-layouts  1.32 us (2%)
  other arithmetic  0.85 us (1%)
    pallas_call x1, Pallas kernels, on_device(): pl.pallas_call(mixed_kernel, out_shape=jax.ShapeDtypeStruct((length, mode...  64.4 us

profile of v4, /device:TPU:256, one launch (start us, length us, event | category | flops | bytes accessed | tf_op | source)
XLA Modules:
  0.0 66.6 jit_solution(16851035347148109913)
XLA Ops:
  0.0 0.8 %multiply_sine_fusion = (f32[32,256]{1,0:T(8,128)}, f32[32,256]{1,0:T(8,128)}) fusion(f32[256]{0:T(256)S(1)} %add_convert_fusion, f32[32]{0:T(128)S(1)} %negate_power_fusion), kind=kLoop, calls=%fused_computation | loop fusion | flops 8192 | bytes 66688 | tf_op jit(solution)/shard_map/sin | solution.py:555
  0.9 64.4 %mixed.1 = bf16[256,4096]{1,0:T(8,128)(2,1)S(1)} custom-call(bf16[256,1024]{1,0:T(8,128)(2,1)} %latent_hbm.1, bf16[256,512]{1,0:T(8,128)(2,1)} %shared_hbm.1, bf16[64,256]{1,0:T(8,128)(2,1)} %bitcast.4, s32[1,256]{1,0:T(1,128)} %bitcast.7, f32[32,256]{1,0:T(8,128)} %get-tuple-element.6.cos_hbm, f32[32,256]{1,0:T(8,128)} %get-tuple-element.5.sin_hbm, ...), custom_call_target="tpu_custom_call" | custom-call | tf_op jit(solution)/shard_map/mixed/pallas_call | solution.py:565
  65.2 1.3 %copy.13 = bf16[256,4096]{1,0:T(8,128)(2,1)} copy(bf16[256,4096]{1,0:T(8,128)(2,1)S(1)} %mixed.1) | data formatting | bytes 4194304
  (2 shorter events, 0.0 us)

commit v5 on v4

--- a/solution.py
+++ b/solution.py
@@ -381,17 +381,15 @@
     steps_of(3, arrived)
     steps_of(4, arrived)
     steps_of(2, finish, absorb_lane)
-    steps_of(1, finish)
+    steps_of(1, finish, absorb_lane)
     steps_of(3, relay)
+    steps_of(2, absorb_sibling)
     steps_of(4, relay)
     for side in (0, 1):
         w_copy(1, side).start()
-    steps_of(1, absorb_lane)
     share(0)
-    steps_of(2, absorb_sibling)
-    steps_of(3, finish)
     steps_of(1, absorb_sibling)
-    steps_of(3, absorb_lane)
+    steps_of(3, finish, absorb_lane)
     steps_of(4, finish, absorb_lane)
     steps_of(3, absorb_sibling)
 

time: 66.7 us -> 66 us (0.990)
  Pallas kernels: 64.4 us -> 63.7 us
    pallas_call x1, Pallas kernels: 64.4 us -> 63.7 us  [on_device(): pl.pallas_call(mixed_kernel, out_shape=jax.ShapeDtypeStruct((length, mode...]
where the time goes in v5:
time: 66 us; the launch traced here: 65.9 us
  Pallas kernels  63.7 us (97%)
  local copies, waits for them, and re-layouts  1.32 us (2%)
  other arithmetic  0.85 us (1%)
    pallas_call x1, Pallas kernels, on_device(): pl.pallas_call(mixed_kernel, out_shape=jax.ShapeDtypeStruct((length, mode...  63.7 us
    unnamed x1, local copies, waits for them, and re-layouts  1.32 us

profile of v5, /device:TPU:256, one launch (start us, length us, event | category | flops | bytes accessed | tf_op | source)
XLA Modules:
  0.0 65.9 jit_solution(5879240693731983446)
XLA Ops:
  0.0 0.8 %multiply_sine_fusion = (f32[32,256]{1,0:T(8,128)}, f32[32,256]{1,0:T(8,128)}) fusion(f32[256]{0:T(256)S(1)} %add_convert_fusion, f32[32]{0:T(128)S(1)} %negate_power_fusion), kind=kLoop, calls=%fused_computation | loop fusion | flops 8192 | bytes 66688 | tf_op jit(solution)/shard_map/sin | solution.py:553
  0.9 63.7 %mixed.1 = bf16[256,4096]{1,0:T(8,128)(2,1)S(1)} custom-call(bf16[256,1024]{1,0:T(8,128)(2,1)} %latent_hbm.1, bf16[256,512]{1,0:T(8,128)(2,1)} %shared_hbm.1, bf16[64,256]{1,0:T(8,128)(2,1)} %bitcast.4, s32[1,256]{1,0:T(1,128)} %bitcast.7, f32[32,256]{1,0:T(8,128)} %get-tuple-element.6.cos_hbm, f32[32,256]{1,0:T(8,128)} %get-tuple-element.5.sin_hbm, ...), custom_call_target="tpu_custom_call" | custom-call | tf_op jit(solution)/shard_map/mixed/pallas_call | solution.py:563
  64.6 1.3 %copy.13 = bf16[256,4096]{1,0:T(8,128)(2,1)} copy(bf16[256,4096]{1,0:T(8,128)(2,1)S(1)} %mixed.1) | data formatting | bytes 4194304
  (2 shorter events, 0.0 us)
